TPU v7x, 32 devices: a whole 2x2x4 slice. The times are simulated.
32 devices in a mesh: sp: 8 (over z, x), tp: 4 (over y, core).
Axes of the slice: x: 2, y: 2, z: 4, core: 2. Of those that a mesh axis runs over, the one named last changes fastest.
Arguments:
- mixer_in: bfloat16 [2048, 2048], P('sp', 'tp'), may hold values from -6 to 6
- doc_ids: int32 [2048], P('sp'), may hold values from 0 to 3, never falling along the last dimension, each value on 1 to 1024 neighbouring positions
- mix_scale: float32 [2048], P('tp'), may hold values from 0.1 to 1.9
- out_proj: bfloat16 [2048, 2048], P('tp'), may hold values from -0.125 to 0.125
- residual: bfloat16 [2048, 2048], P('sp'), may hold values from -6 to 6
- mix_gain: float32 [2048], replicated, may hold values from 0.1 to 1.9
- expert_ids: int32 [2048, 2], P('sp'), may hold values from 0 to 7, all different within a row; in each aligned block of 256 rows (0 to 255, 256 to 511, ...) at most 128 rows name the same one
- expert_weight: float32 [2048, 2], P('sp'), may hold values from 0.2 to 1
- w_gate: bfloat16 [8, 2048, 5632], P('sp', None, 'tp'), may hold values from -0.125 to 0.125
- w_up: bfloat16 [8, 2048, 5632], P('sp', None, 'tp'), may hold values from -0.125 to 0.125
- w_down: bfloat16 [8, 5632, 2048], P('sp', 'tp'), may hold values from -0.078125 to 0.078125
- out_gain: float32 [2048], replicated, may hold values from 0.1 to 1.9
Outputs:
- layer_out: bfloat16 [2048, 2048], P('sp')
Inputs may be any that keep to these rules, and one draw needn't show every extreme that they name: `doc_ids`: document numbers never fall along the tokens; a document has at most 1024 positions. `expert_ids`: A row's two experts differ. In each aligned block of 256 rows (the tokens of one index of sp) no expert is named by more than 128 rows; some block has an expert named by exactly 128 rows.
All inputs are finite; a program needn't handle non-finite values.
Results may differ from a plain program's by a relative error of at most 0.015.
Values may be sent and summed in bfloat16 or wider, within the bound.
No kernel may reach another device: no remote copies, remote signals or barrier semaphores. Data moves between devices by JAX's collectives and lax.ppermute only.
A program may use at most 64 MiB of HBM per device.

v0:
```python
import jax
import jax.numpy as jnp
from jax import lax
from jax.sharding import PartitionSpec as P

alpha_res = 1.4142135623730951
norm_eps = 1e-05
pool_reach = 15


def passed_along(value, axis, steps):
    count = lax.axis_size(axis)
    initial, last = (max(0, -steps), min(count, count - steps))
    return lax.ppermute(value, axis, [(source, source + steps) for source in range(initial, last)])


def layer_norm(summed, norm_gain):
    row_mean = jnp.mean(summed, axis=-1, keepdims=True)
    centred = summed - row_mean
    row_var = jnp.mean(centred * centred, axis=-1, keepdims=True)
    return centred * lax.rsqrt(row_var + norm_eps) * norm_gain


def pair_slots(pair_ids, experts):
    flat_ids = pair_ids.reshape(-1)
    onehot = (flat_ids[:, None] == jnp.arange(experts, dtype=jnp.int32)[None, :]).astype(jnp.int32)
    before = jnp.cumsum(onehot, axis=0) - onehot
    return jnp.sum(before * onehot, axis=1).reshape(pair_ids.shape)


def shards(
    mixer_in,
    doc_ids,
    mix_scale,
    out_proj,
    residual,
    mix_gain,
    expert_ids,
    expert_weight,
    w_gate,
    w_up,
    w_down,
    out_gain,
):
    tok_rows, chan_cols = mixer_in.shape
    features = mix_gain.shape[0]
    tail_rows = (mixer_in[tok_rows - pool_reach :], doc_ids[tok_rows - pool_reach :])
    before_vals, before_doc = passed_along((tail_rows[0], tail_rows[1]), "sp", 1)
    extended = jnp.concatenate([before_vals, mixer_in], axis=0).astype(jnp.float32)
    extended_doc = jnp.concatenate([before_doc, doc_ids], axis=0)
    positions = lax.axis_index("sp") * tok_rows + jnp.arange(tok_rows, dtype=jnp.int32)
    channel = lax.axis_index("tp") * chan_cols + jnp.arange(chan_cols, dtype=jnp.int32)
    window = jnp.left_shift(jnp.int32(2), channel // (features // 4))
    window_sum = jnp.zeros((tok_rows, chan_cols), jnp.float32)
    window_count = jnp.zeros((tok_rows, chan_cols), jnp.float32)
    for lag_step in range(pool_reach + 1):
        shifted = extended[pool_reach - lag_step : pool_reach - lag_step + tok_rows]
        same_doc = (
            extended_doc[pool_reach - lag_step : pool_reach - lag_step + tok_rows] == doc_ids
        ) & (positions >= lag_step)
        in_window = (same_doc[:, None] & (lag_step < window)[None, :]).astype(jnp.float32)
        window_sum = window_sum + in_window * shifted
        window_count = window_count + in_window
    mixed_rows = ((window_sum / window_count - extended[pool_reach:]) * mix_scale).astype(
        jnp.bfloat16
    )
    share_rows = tok_rows // lax.axis_size("tp")
    projected = lax.psum_scatter(
        jnp.dot(mixed_rows, out_proj, preferred_element_type=jnp.float32).astype(jnp.bfloat16),
        "tp",
        scatter_dimension=0,
        tiled=True,
    ).astype(jnp.float32)
    own_residual = lax.dynamic_slice_in_dim(
        residual, lax.axis_index("tp") * share_rows, share_rows, 0
    )
    normed_share = layer_norm(
        alpha_res * own_residual.astype(jnp.float32) + projected, mix_gain
    ).astype(jnp.bfloat16)
    normed = lax.all_gather(normed_share, "tp", axis=0, tiled=True)
    experts = lax.axis_size("sp")
    capacity = 4 * tok_rows // experts
    ranks = pair_slots(expert_ids, experts)
    target = expert_ids * capacity + ranks
    slot_ids = jnp.arange(experts * capacity, dtype=jnp.int32)[:, None]
    select = ((target[None, :, 0] == slot_ids) | (target[None, :, 1] == slot_ids)).astype(
        jnp.bfloat16
    )
    source_rows = lax.dynamic_slice_in_dim(normed, lax.axis_index("tp") * chan_cols, chan_cols, 1)
    outgoing = jnp.dot(select, source_rows, preferred_element_type=jnp.float32).astype(jnp.bfloat16)
    outgoing = outgoing.reshape(experts, capacity, source_rows.shape[1])
    incoming = lax.all_to_all(outgoing, "sp", split_axis=0, concat_axis=0, tiled=True)
    incoming = lax.all_gather(incoming, "tp", axis=2, tiled=True)
    senders, slot_count, width_all = incoming.shape
    flat_in = incoming.reshape(senders * slot_count, width_all)
    gate_pre = jnp.dot(flat_in, w_gate[0], preferred_element_type=jnp.float32)
    upper = jnp.dot(flat_in, w_up[0], preferred_element_type=jnp.float32)
    hidden = (jax.nn.silu(gate_pre) * upper).astype(jnp.bfloat16)
    partial_value = jnp.dot(hidden, w_down[0], preferred_element_type=jnp.float32).astype(
        jnp.bfloat16
    )
    returned = lax.all_to_all(
        partial_value.reshape(senders, slot_count, width_all),
        "sp",
        split_axis=0,
        concat_axis=0,
        tiled=True,
    )
    picked = returned.reshape(experts * capacity, features)[target]
    weighted = jnp.sum(picked.astype(jnp.float32) * expert_weight[:, :, None], axis=1)
    routed = lax.psum(weighted.astype(jnp.bfloat16), "tp").astype(jnp.float32)
    return layer_norm(alpha_res * normed.astype(jnp.float32) + routed, out_gain).astype(
        jnp.bfloat16
    )


def solution(mesh):
    placed = (
        P("sp", "tp"),
        P("sp"),
        P("tp"),
        P("tp", None),
        P("sp", None),
        P(),
        P("sp", None),
        P("sp", None),
        P("sp", None, "tp"),
        P("sp", None, "tp"),
        P("sp", "tp", None),
        P(),
    )
    return jax.shard_map(
        shards, mesh=mesh, in_specs=placed, out_specs=P("sp", None), check_vma=False
    )
```

profile of v0, /device:TPU:0, one launch (start us, length us, event | category | flops | bytes accessed | tf_op | source)
XLA Modules:
  0.0 340.1 jit_solution(10196914106169270172)
XLA Ops:
  6.5 0.0 copy-start
  6.5 0.0 reduce-scatter.2.cloned.1.call-start
  6.5 0.9 slice.114
  7.4 4.9 %collective-permute-start.1 = (s32[15]{0:T(128)S(1)}, s32[15]{0:T(128)S(1)}, u32[]{:S(2)}, u32[]{:S(2)}) collective-permute-start(s32[15]{0:T(128)S(1)} %slice.114), channel_id=1, source_target_pairs={{0,4},{4,8},{8,12},{12,16},{16,20},{20,24},{24,28},{1,5},{5,9},{9,... | collective-permute-start | bytes 188 | tf_op jit(solution)/shard_map/ppermute | solution.py:14
  12.3 0.7 slice.112
  13.0 3.4 %collective-permute-start = (bf16[15,512]{1,0:T(8,128)(2,1)S(1)}, bf16[15,512]{1,0:T(8,128)(2,1)S(1)}, u32[]{:S(2)}, u32[]{:S(2)}) collective-permute-start(bf16[15,512]{1,0:T(8,128)(2,1)S(1)} %slice.112), channel_id=1, source_target_pairs={{0,4},{4,8},{8,12},{12,16},{16,20},{20,24},{24,28},{1,5},{5,9},{9,... | collective-permute-start | bytes 46088 | tf_op jit(solution)/shard_map/ppermute | solution.py:14
  16.7 0.0 collective-permute-done.1
  16.7 0.8 pad_add_fusion
  17.4 0.8 compare_and_fusion.14
  18.2 0.0 collective-permute-done
  18.2 1.0 maximum_convert_fusion
  19.2 0.0 copy-done
  19.2 0.0 copy-start.3
  19.3 0.0 copy-start.4
  19.3 0.0 copy-start.6
  19.3 5.9 %convolution_convert_fusion = bf16[256,2048]{1,0:T(8,128)(2,1)} fusion(bf16[512,2048]{1,0:T(8,128)(2,1)S(1)} %copy-done, f32[271,512]{1,0:T(8,128)S(1)} %maximum_convert_fusion, f32[512]{0:T(512)} %param.14, pred[512]{0:T(512)(128)(4,1)S(1)} %get-tuple-element.24, pred[512]{0:T(512)(128)(4,1)S(1)} %get-tuple-element.25, ...), kind=kOutput, calls=%fused_computation.11 | convolution fusion | flops 548143104 | bytes 11552768 | tf_op jit(solution)/shard_map/dot_general | solution.py:69
  25.2 0.0 reduce-scatter.2.cloned.1.call-update
  25.2 0.0 all-gather.3.cloned.1.call-start
  25.3 26.5 %reduce-scatter.2.cloned.1.call-done = bf16[64,2048]{1,0:T(8,128)(2,1)} async-done(((bf16[256,2048]{1,0:T(8,128)(2,1)}), bf16[64,2048]{1,0:T(8,128)(2,1)}) %reduce-scatter.2.cloned.1.call-update) | async-done | bytes 262160 | tf_op jit(solution)/shard_map/reduce_scatter | solution.py:68
  51.8 0.0 copy-done.3
  51.8 1.1 fusion.53
  53.0 1.2 multiply_reduce_fusion.2
  54.2 0.0 copy-done.4
  54.2 1.8 multiply_convert_fusion.2
  56.0 0.0 all-gather.3.cloned.1.call-update
  56.0 0.0 all-gather.5.cloned.1.call-start
  56.0 0.0 copy-done.6
  56.1 0.1 copy.24
  56.2 0.1 eq.119
  56.3 0.1 eq.115
  56.5 1.1 reduce-window.6
  57.6 0.2 slice_reduce_fusion
  57.9 0.1 fusion.56
  58.0 0.1 reshape.149
  58.2 0.1 copy.26
  58.2 14.7 %all-gather.3.cloned.1.call-done = bf16[256,2048]{1,0:T(8,128)(2,1)} async-done(((bf16[64,2048]{1,0:T(8,128)(2,1)}), bf16[256,2048]{1,0:T(8,128)(2,1)}) %all-gather.3.cloned.1.call-update) | async-done | bytes 1048592 | tf_op jit(solution)/shard_map/all_gather | solution.py:80
  72.9 1.4 convolution_convert_fusion.1
  74.3 31.5 %all_to_all.10 = bf16[8,128,512]{2,1,0:T(8,128)(2,1)} all-to-all(bf16[8,128,512]{2,1,0:T(8,128)(2,1)S(1)} %bitcast.35), channel_id=1, replica_groups=mesh['sp'=8,'tp'=4] {'sp'}, dimensions={0} | all-to-all | bytes 2097152 | tf_op jit(solution)/shard_map/all_to_all | solution.py:92
  105.8 0.0 all-gather.5.cloned.1.call-update
  105.9 32.7 %all-gather.5.cloned.1.call-done = bf16[8,128,2048]{2,1,0:T(8,128)(2,1)} async-done(((bf16[8,128,512]{2,1,0:T(8,128)(2,1)}), bf16[8,128,2048]{2,1,0:T(8,128)(2,1)}) %all-gather.5.cloned.1.call-update) | async-done | bytes 4194320 | tf_op jit(solution)/shard_map/all_gather | solution.py:93
  138.6 11.7 %fusion.4 = f32[1024,1408]{1,0:T(8,128)} fusion(bf16[1024,2048]{1,0:T(8,128)(2,1)} %bitcast.38, bf16[1,2048,1408]{2,1,0:T(8,128)(2,1)} %param.20), kind=kOutput, calls=%fused_computation.5 | convolution fusion | flops 5905580032 | bytes 15728640 | tf_op jit(solution)/shard_map/dot_general | solution.py:96
  150.3 20.6 %fusion.10 = bf16[1024,2048]{1,0:T(8,128)(2,1)} fusion(bf16[1,1408,2048]{2,1,0:T(8,128)(2,1)} %param.22, f32[1024,1408]{1,0:T(8,128)} %fusion.4, bf16[1024,2048]{1,0:T(8,128)(2,1)} %bitcast.39, bf16[1,2048,1408]{2,1,0:T(8,128)(2,1)} %param.21), kind=kOutput, calls=%fused_computation.9 | convolution fusion | flops 11821907968 | bytes 25690112 | tf_op jit(solution)/shard_map/dot_general | solution.py:99
  171.0 0.0 copy-start.7
  171.0 5.6 %all-to-all-start.1 = ((bf16[8,128,2048]{2,1,0:T(8,128)(2,1)}), bf16[8,128,2048]{2,1,0:T(8,128)(2,1)}, u32[]{:S(2)}, u32[]{:S(2)}) async-start(bf16[8,128,2048]{2,1,0:T(8,128)(2,1)} %bitcast.34), calls=%async_computation.2 | async-start | bytes 8388608 | tf_op jit(solution)/shard_map/all_to_all | solution.py:102
  176.6 0.0 all-reduce.2.cloned.1.call-start
  176.7 0.1 copy.27
  176.8 0.1 reshape.156
  177.0 0.0 copy-done.7
  177.0 0.1 copy.28
  177.1 93.2 %all-to-all-done.1 = bf16[8,128,2048]{2,1,0:T(8,128)(2,1)} async-done(((bf16[8,128,2048]{2,1,0:T(8,128)(2,1)}), bf16[8,128,2048]{2,1,0:T(8,128)(2,1)}, u32[]{:S(2)}, u32[]{:S(2)}) %all-to-all-start.1) | async-done | bytes 4194336 | tf_op jit(solution)/shard_map/all_to_all | solution.py:102
  270.3 8.2 %gather_fusion = bf16[512,2048]{1,0:T(8,128)(2,1)} fusion(bf16[1024,2048]{1,0:T(8,128)(2,1)} %bitcast.10, s32[1024]{0:T(1024)S(1)} %pad_clamp_fusion), kind=kCustom, calls=%fused_computation | custom fusion | bytes 4196352 | tf_op jit(solution)/shard_map/gather | solution.py:109
  278.5 5.4 %reshape.164 = f32[256,2,2048]{2,1,0:T(2,128)} reshape(bf16[512,2048]{1,0:T(8,128)(2,1)} %gather_fusion) | data formatting | bytes 6291456 | tf_op jit(solution)/shard_map/convert_element_type | solution.py:110
  283.9 0.0 copy-start.1
  283.9 0.0 copy-start.5
  283.9 9.9 %multiply_reduce_fusion = bf16[256,2048]{1,0:T(8,128)(2,1)} fusion(f32[256,2,2048]{2,1,0:T(2,128)} %reshape.164, f32[256,2]{1,0:T(8,128)S(1)} %copy.28), kind=kLoop, calls=%fused_computation.8 | loop fusion | flops 1572864 | bytes 5244928 | tf_op jit(solution)/shard_map/reduce_sum | solution.py:110
  293.9 0.0 all-reduce.2.cloned.1.call-update
  293.9 34.6 %all-reduce.2.cloned.1.call-done = bf16[256,2048]{1,0:T(8,128)(2,1)} async-done(((bf16[256,2048]{1,0:T(8,128)(2,1)}), bf16[256,2048]{1,0:T(8,128)(2,1)}) %all-reduce.2.cloned.1.call-update) | async-done | bytes 1048592 | tf_op jit(solution)/shard_map/psum | solution.py:111
  328.4 0.0 copy-done.1
  328.4 0.0 copy-start.2
  328.5 1.7 fusion.16
  330.2 1.8 multiply_reduce_fusion.1
  332.0 0.0 copy-done.5
  332.0 0.0 copy-done.2
  332.0 1.5 multiply_convert_fusion.1
  (18 shorter events, 0.2 us)
Async XLA Ops:
  6.5 12.7 %copy-start = (bf16[512,2048]{1,0:T(8,128)(2,1)S(1)}, bf16[512,2048]{1,0:T(8,128)(2,1)}, u32[]{:S(2)}) copy-start(bf16[512,2048]{1,0:T(8,128)(2,1)} %param.15) | copy-start | bytes 6291460
  6.5 45.3 %reduce-scatter.2.cloned.1.call-start = ((), (), s32[]{:S(2)}) async-start(), calls=%async_computation.3 | async-start | bytes 1310720 | tf_op jit(solution)/shard_map/reduce_scatter | solution.py:68
  7.4 9.2 %collective-permute-start.1 = (s32[15]{0:T(128)S(1)}, s32[15]{0:T(128)S(1)}, u32[]{:S(2)}, u32[]{:S(2)}) collective-permute-start(s32[15]{0:T(128)S(1)} %slice.114), channel_id=1, source_target_pairs={{0,4},{4,8},{8,12},{12,16},{16,20},{20,24},{24,28},{1,5},{5,9},{9,... | collective-permute-start | bytes 188 | tf_op jit(solution)/shard_map/ppermute | solution.py:14
  13.0 5.2 %collective-permute-start = (bf16[15,512]{1,0:T(8,128)(2,1)S(1)}, bf16[15,512]{1,0:T(8,128)(2,1)S(1)}, u32[]{:S(2)}, u32[]{:S(2)}) collective-permute-start(bf16[15,512]{1,0:T(8,128)(2,1)S(1)} %slice.112), channel_id=1, source_target_pairs={{0,4},{4,8},{8,12},{12,16},{16,20},{20,24},{24,28},{1,5},{5,9},{9,... | collective-permute-start | bytes 46088 | tf_op jit(solution)/shard_map/ppermute | solution.py:14
  19.2 32.6 %copy-start.3 = (bf16[256,2048]{1,0:T(8,128)(2,1)S(1)}, bf16[256,2048]{1,0:T(8,128)(2,1)}, u32[]{:S(2)}) copy-start(bf16[256,2048]{1,0:T(8,128)(2,1)} %param.16) | copy-start | bytes 3145732
  19.3 34.9 %copy-start.4 = (f32[2048]{0:T(1024)S(1)}, f32[2048]{0:T(1024)}, u32[]{:S(2)}) copy-start(f32[2048]{0:T(1024)} %param.17) | copy-start | bytes 24580
  19.3 36.8 %copy-start.6 = (s32[256,2]{0,1:T(2,128)S(1)}, s32[256,2]{0,1:T(2,128)}, u32[]{:S(2)}) copy-start(s32[256,2]{0,1:T(2,128)} %param.18) | copy-start | bytes 6148
  25.2 47.7 %all-gather.3.cloned.1.call-start = ((), (), s32[]{:S(2)}) async-start(), calls=%async_computation.4 | async-start | bytes 1310720 | tf_op jit(solution)/shard_map/all_gather | solution.py:80
  56.0 82.6 %all-gather.5.cloned.1.call-start = ((), (), s32[]{:S(2)}) async-start(), calls=%async_computation.5 | async-start | bytes 5242880 | tf_op jit(solution)/shard_map/all_gather | solution.py:93
  171.0 6.0 %copy-start.7 = (f32[256,2]{0,1:T(2,128)S(1)}, f32[256,2]{0,1:T(2,128)}, u32[]{:S(2)}) copy-start(f32[256,2]{0,1:T(2,128)} %param.19) | copy-start | bytes 6148
  171.0 99.3 %all-to-all-start.1 = ((bf16[8,128,2048]{2,1,0:T(8,128)(2,1)}), bf16[8,128,2048]{2,1,0:T(8,128)(2,1)}, u32[]{:S(2)}, u32[]{:S(2)}) async-start(bf16[8,128,2048]{2,1,0:T(8,128)(2,1)} %bitcast.34), calls=%async_computation.2 | async-start | bytes 8388608 | tf_op jit(solution)/shard_map/all_to_all | solution.py:102
  176.6 151.8 %all-reduce.2.cloned.1.call-start = ((), (), s32[]{:S(2)}) async-start(), calls=%async_computation.6 | async-start | bytes 2097152 | tf_op jit(solution)/shard_map/psum | solution.py:111
  283.9 44.5 %copy-start.1 = (bf16[256,2048]{1,0:T(8,128)(2,1)S(1)}, bf16[256,2048]{1,0:T(8,128)(2,1)}, u32[]{:S(2)}) copy-start(bf16[256,2048]{1,0:T(8,128)(2,1)} %all-gather.3.cloned.1.call-done) | copy-start | bytes 3145732
  283.9 48.1 %copy-start.5 = (f32[2048]{0:T(1024)S(1)}, f32[2048]{0:T(1024)}, u32[]{:S(2)}) copy-start(f32[2048]{0:T(1024)} %param.23) | copy-start | bytes 24580
  328.4 3.5 %copy-start.2 = (bf16[256,2048]{1,0:T(8,128)(2,1)S(1)}, bf16[256,2048]{1,0:T(8,128)(2,1)}, u32[]{:S(2)}) copy-start(bf16[256,2048]{1,0:T(8,128)(2,1)} %all-reduce.2.cloned.1.call-done) | copy-start | bytes 3145732
Sparse Core Ops, SparseCore 0:
  25.3 26.4 reduce-scatter.1
  56.1 16.7 all-gather.2
  106.0 32.5 all-gather.4
  294.0 34.4 all-reduce.1
where the time goes:
time: 341 us; the launch traced here: 340 us
  waiting for transfers between devices  202 us (59%)
  matrix products  39.7 us (12%)
  blocking collectives  31.5 us (9%)
  other arithmetic  23.1 us (7%)
  local copies, waits for them, and re-layouts  16.5 us (5%)
  starting transfers between devices  14.1 us (4%)
  between operations  13.4 us (4%)
    all_to_all x1, waiting for transfers between devices, shards(): lax.all_to_all(partial_value.reshape(senders, slot_count, width_all), 'sp...  93.2 us
    psum x1, waiting for transfers between devices, shards(): routed = lax.psum(weighted.astype(jnp.bfloat16), 'tp').astype(jnp.float32)  34.6 us
    all_gather x1, waiting for transfers between devices, shards(): incoming = lax.all_gather(incoming, 'tp', axis=2, tiled=True)  32.7 us
    all_to_all x1, blocking collectives, shards(): lax.all_to_all(outgoing, 'sp', split_axis=0, concat_axis=0, tiled=True)  31.5 us
    reduce_scatter x1, waiting for transfers between devices, shards(): lax.psum_scatter(jnp.dot(mixed_rows, out_proj, preferred_element_type=jnp...  26.5 us
    dot_general x1, matrix products, shards(): jnp.dot(hidden, w_down[0], preferred_element_type=jnp.float32)  20.6 us
    all_gather x1, waiting for transfers between devices, shards(): normed = lax.all_gather(normed_share, 'tp', axis=0, tiled=True)  14.7 us
    dot_general x1, matrix products, shards(): gate_pre = jnp.dot(flat_in, w_gate[0], preferred_element_type=jnp.float32)  11.7 us
  transfers between devices with their start and end apart: 7, of which 5 were waited for; matrix products, arithmetic and copies ran while one was open for 1% of the time, Pallas kernels for 0%

commit v1 on v0

v1 whole, which is shorter than its diff:
```python
import functools

import jax
import jax.numpy as jnp
from jax import lax
from jax.experimental import pallas as pl
from jax.experimental.pallas import tpu as pltpu
from jax.sharding import PartitionSpec as P

alpha_res = 1.4142135623730951
norm_eps = 1e-05
reach = 16
lanes = 128
f32, bf16 = jnp.float32, jnp.bfloat16
MIB = 2**20


def swap(value, axis, bits):
    if bits == 0:
        return value
    count = lax.axis_size(axis)
    return lax.ppermute(value, axis, [(i, i ^ bits) for i in range(count)])


def tiles(total, width):
    return [(at, min(width, total - at)) for at in range(0, total, width)]


def dot(a, b):
    return jnp.dot(a, b, preferred_element_type=f32)


def call(body, outs, operands, scratch=(), flops=1_000_000, vmem=16, name=None):
    whole = pl.BlockSpec(memory_space=pltpu.VMEM)
    return pl.pallas_call(
        body,
        out_shape=[jax.ShapeDtypeStruct(shape, kind) for shape, kind in outs],
        in_specs=[whole] * len(operands),
        out_specs=[whole] * len(outs),
        scratch_shapes=list(scratch),
        compiler_params=pltpu.CompilerParams(vmem_limit_bytes=vmem * MIB),
        cost_estimate=pl.CostEstimate(flops=flops, bytes_accessed=0, transcendentals=0),
        name=name,
    )(*operands)


def place():
    t = lax.axis_index("tp")
    return t & 1, t >> 1, lax.axis_size("tp") // 2


def columns(start, width):
    return pl.ds(pl.multiple_of(start, lanes), width)


def as_column(row):
    return jnp.broadcast_to(row, (lanes, row.shape[1])).T[:, :1]


def tail_body(x, docs, pack):
    rows = x.shape[0]
    pack[0:reach, :] = x[rows - reach :, :]
    pack[reach:, :] = jnp.zeros_like(pack[reach:, :])
    pack[reach:, 0:lanes] = jnp.broadcast_to(
        docs[:, rows - lanes :].astype(f32), (reach, lanes)
    ).astype(bf16)


def mix_body(x, pack, docs, scale, weights, keep, send):
    core, _, _ = place()
    rows, cols = x.shape
    half = keep.shape[1]
    window = jnp.left_shift(2, lax.axis_index("tp") * cols // (2 * half // 4))
    doc_row = docs[...].astype(f32)
    doc_col = as_column(doc_row)
    lag = lax.broadcasted_iota(jnp.int32, (rows, rows), 0) - lax.broadcasted_iota(
        jnp.int32, (rows, rows), 1
    )
    band = jnp.where((lag >= 0) & (lag < window) & (doc_col == doc_row), 1.0, 0.0)
    total = dot(band.astype(bf16), x[...])
    count = jnp.sum(band, axis=1, keepdims=True)
    lag_tail = (
        lax.broadcasted_iota(jnp.int32, (reach, lanes), 0)
        + lanes
        - lax.broadcasted_iota(jnp.int32, (reach, lanes), 1)
    )
    tail_doc = pack[reach : reach + 1, 0:lanes].astype(f32)
    inside = (lag_tail < window) & (doc_col[:reach] == tail_doc) & (lax.axis_index("sp") > 0)
    band_tail = jnp.where(inside, 1.0, 0.0)
    before = jnp.concatenate(
        [jnp.zeros((lanes - reach, cols), bf16), pack[0:reach, :]], axis=0
    )
    top = total[:reach] + dot(band_tail.astype(bf16), before)
    top_count = count[:reach] + jnp.sum(band_tail, axis=1, keepdims=True)
    total = jnp.concatenate([top, total[reach:]], axis=0)
    count = jnp.concatenate([top_count, count[reach:]], axis=0)
    mixed = ((total / count - x[...].astype(f32)) * scale[...]).astype(bf16)
    for out, which in ((send, 1 - core), (keep, core)):
        for at, width in tiles(half, 256):
            out[:, at : at + width] = dot(
                mixed, weights[:, columns(which * half + at, width)]
            ).astype(out.dtype)


def split_body(keep, arrived, own, *sends):
    _, y, _ = place()
    part = own.shape[1]
    for bits, out in enumerate((own, *sends)):
        at = columns((y ^ bits) * part, part)
        out[...] = (keep[:, at].astype(f32) + arrived[:, at].astype(f32)).astype(out.dtype)


def stats_body(parts, *refs):
    own, arrived, residual, z_out, stats = refs[0], refs[1:parts], refs[parts], refs[-2], refs[-1]
    core, y, y_parts = place()
    width = own.shape[1]
    z = alpha_res * residual[:, columns((core * y_parts + y) * width, width)].astype(f32)
    shares = own[...]
    for ref in arrived:
        shares = shares + ref[...].astype(f32)
    z = z + shares
    z_out[...] = z
    mean = jnp.mean(z, axis=1, keepdims=True)
    spread = jnp.sum((z - mean) * (z - mean), axis=1, keepdims=True)
    lane = lax.broadcasted_iota(jnp.int32, (z.shape[0], lanes), 1)
    stats[...] = jnp.where(lane == 0, mean, spread).T[0:8, :]


def slot_rows(ids, capacity, experts):
    tokens = ids.shape[1]
    expert = lax.broadcasted_iota(jnp.int32, (experts, tokens), 0)
    first, second = expert == ids[0:1, :], expert == ids[1:2, :]
    named = jnp.where(first | second, 1.0, 0.0)
    earlier = (
        lax.broadcasted_iota(jnp.int32, (tokens, tokens), 0)
        < lax.broadcasted_iota(jnp.int32, (tokens, tokens), 1)
    )
    before = dot(named.astype(bf16), jnp.where(earlier, 1.0, 0.0).astype(bf16))
    slots = []
    for k, mine in enumerate((first, second)):
        rank = jnp.sum(jnp.where(mine, before, 0.0), axis=0, keepdims=True)
        slots.append(ids[k : k + 1, :] * capacity + rank.astype(jnp.int32))
    return slots


def dispatch_body(devices, experts, *refs):
    stats, (z_ref, gain, ids), outs = refs[:devices], refs[devices : devices + 3], refs[devices + 3 :]
    normed_ref, sends = outs[0], outs[1:]
    core, y, y_parts = place()
    tokens, width = z_ref.shape
    capacity = sends[0].shape[0]
    means = [ref[0:1, :] for ref in stats]
    mean = sum(means[1:], means[0]) / devices
    spread = sum(
        (ref[1:2, :] + width * (m - mean) * (m - mean) for ref, m in zip(stats, means)),
        jnp.zeros_like(mean),
    )
    scale = lax.rsqrt(spread / (width * devices) + norm_eps)
    gain_here = gain[:, columns((core * y_parts + y) * width, width)]
    normed = (z_ref[...] - as_column(mean)) * as_column(scale) * gain_here
    normed = normed.astype(bf16)
    normed_ref[...] = normed
    slots = slot_rows(ids, capacity, experts)
    s = lax.axis_index("sp")
    for bits, out in enumerate(sends):
        slot = (s ^ bits) * capacity + lax.broadcasted_iota(jnp.int32, (capacity, tokens), 0)
        chosen = jnp.where((slots[0] == slot) | (slots[1] == slot), 1.0, 0.0)
        out[...] = dot(chosen.astype(bf16), normed).astype(bf16)


def stack_body(*refs):
    out = refs[-1]
    rows = refs[0].shape[0]
    for i, ref in enumerate(refs[:-1]):
        out[i * rows : (i + 1) * rows, :] = ref[...]


def unpack(pieces, wide):
    core, y, y_parts = place()
    width = pieces[0].shape[1]
    for i, ref in enumerate(pieces):
        at = (core ^ (i // y_parts)) * y_parts + (y ^ (i % y_parts))
        wide[:, columns(at * width, width)] = ref[...]


def expert_body(count, *refs):
    pieces, (w_gate, w_up, w_down), (send, keep) = (
        refs[:count],
        refs[count : count + 3],
        refs[count + 3 : count + 5],
    )
    wide, hidden = refs[count + 5 :]
    core, _, _ = place()
    unpack(pieces, wide)
    half = keep.shape[1]
    for at, width in tiles(w_gate.shape[1], 256):
        gate = dot(wide[...], w_gate[:, at : at + width])
        upper = dot(wide[...], w_up[:, at : at + width])
        hidden[:, at : at + width] = (gate / (1.0 + jnp.exp(-gate)) * upper).astype(bf16)
    for out, which in ((send, 1 - core), (keep, core)):
        for at, width in tiles(half, 256):
            out[:, at : at + width] = dot(
                hidden[...], w_down[:, columns(which * half + at, width)]
            ).astype(bf16)


def homeward_body(parts, *refs):
    own, arrived, outs = refs[0], refs[1:parts], refs[parts:]
    rows = outs[0].shape[0]
    total = own[...].astype(f32)
    for ref in arrived:
        total = total + ref[...].astype(f32)
    for i, out in enumerate(outs):
        out[...] = total[i * rows : (i + 1) * rows].astype(bf16)


def combine_body(experts, *refs):
    returned, (ids, pair_weight, normed, z_out) = refs[:experts], refs[experts:]
    capacity = returned[0].shape[0]
    tokens = normed.shape[0]
    slots = slot_rows(ids, capacity, experts)
    s = lax.axis_index("sp")
    z = alpha_res * normed[...].astype(f32)
    for bits, ref in enumerate(returned):
        slot = (s ^ bits) * capacity + lax.broadcasted_iota(jnp.int32, (capacity, tokens), 0)
        chosen = jnp.where(slots[0] == slot, pair_weight[0:1, :], 0.0) + jnp.where(
            slots[1] == slot, pair_weight[1:2, :], 0.0
        )
        high = chosen.astype(bf16)
        low = (chosen - high.astype(f32)).astype(bf16)
        for share in (high, low):
            z = z + lax.dot_general(
                share, ref[...], (((0,), (0,)), ((), ())), preferred_element_type=f32
            )
    z_out[...] = z.astype(bf16)


def norm_body(*refs):
    pieces, gain, out, wide = refs[:-3], refs[-3], refs[-2], refs[-1]
    unpack(pieces, wide)
    z = wide[...].astype(f32)
    centred = z - jnp.mean(z, axis=1, keepdims=True)
    var = jnp.mean(centred * centred, axis=1, keepdims=True)
    out[...] = (centred * lax.rsqrt(var + norm_eps) * gain[...]).astype(bf16)


def over_tp(value, y_parts):
    mine = [swap(value, "tp", bits << 1) for bits in range(y_parts)]
    return mine + [swap(part, "tp", 1) for part in mine]


def shards(
    mixer_in,
    doc_ids,
    mix_scale,
    out_proj,
    residual,
    mix_gain,
    expert_ids,
    expert_weight,
    w_gate,
    w_up,
    w_down,
    out_gain,
):
    tokens, cols = mixer_in.shape
    features = mix_gain.shape[0]
    experts, devices = lax.axis_size("sp"), lax.axis_size("tp")
    y_parts = devices // 2
    half, part = features // 2, features // devices
    capacity = 4 * tokens // experts
    docs = doc_ids.reshape(1, tokens)
    ids, pair_weight = expert_ids.T, expert_weight.T

    (pack,) = call(tail_body, [((2 * reach, cols), bf16)], (mixer_in, docs), name="tail")
    pack = lax.ppermute(pack, "sp", [(i, i + 1) for i in range(experts - 1)])
    keep, send = call(
        mix_body,
        [((tokens, half), f32), ((tokens, half), bf16)],
        (mixer_in, pack, docs, mix_scale.reshape(1, cols), out_proj),
        flops=2 * tokens * cols * features,
        name="mix",
    )
    arrived = swap(send, "tp", 1)
    own, *sends = call(
        split_body,
        [((tokens, part), f32)] + [((tokens, part), bf16)] * (y_parts - 1),
        (keep, arrived),
        name="split",
    )
    shares = [swap(v, "tp", (i + 1) << 1) for i, v in enumerate(sends)]
    z, stats = call(
        functools.partial(stats_body, y_parts),
        [((tokens, part), f32), ((8, tokens), f32)],
        (own, *shares, residual),
        name="stats",
    )
    every = [swap(stats, "tp", bits) for bits in range(devices)]
    normed, *outgoing = call(
        functools.partial(dispatch_body, devices, experts),
        [((tokens, part), bf16)] + [((capacity, part), bf16)] * experts,
        (*every, z, mix_gain.reshape(1, features), ids),
        flops=2 * tokens * tokens * part * 4,
        name="dispatch",
    )
    incoming = [swap(v, "sp", bits) for bits, v in enumerate(outgoing)]
    group = experts // 2
    rows = group * capacity
    returned = []
    for first in range(0, experts, group):
        (stacked,) = call(
            stack_body, [((rows, part), bf16)], incoming[first : first + group], name="stack"
        )
        pieces = over_tp(stacked, y_parts)
        send, keep = call(
            functools.partial(expert_body, len(pieces)),
            [((rows, half), bf16)] * 2,
            (*pieces, w_gate[0], w_up[0], w_down[0]),
            scratch=[
                pltpu.VMEM((rows, features), bf16),
                pltpu.VMEM((rows, w_gate.shape[2]), bf16),
            ],
            flops=6 * rows * features * w_gate.shape[2],
            vmem=24,
            name="expert",
        )
        arrived = swap(send, "tp", 1)
        own, *sends = call(
            split_body,
            [((rows, part), bf16)] * y_parts,
            (keep, arrived),
            name="part",
        )
        shares = [swap(v, "tp", (i + 1) << 1) for i, v in enumerate(sends)]
        homeward = call(
            functools.partial(homeward_body, y_parts),
            [((capacity, part), bf16)] * group,
            (own, *shares),
            name="homeward",
        )
        returned += [swap(v, "sp", first + i) for i, v in enumerate(homeward)]
    (z,) = call(
        functools.partial(combine_body, experts),
        [((tokens, part), bf16)],
        (*returned, ids, pair_weight, normed),
        flops=4 * tokens * experts * capacity * part,
        name="combine",
    )
    (out,) = call(
        norm_body,
        [((tokens, features), bf16)],
        (*over_tp(z, y_parts), out_gain.reshape(1, features)),
        scratch=[pltpu.VMEM((tokens, features), bf16)],
        name="norm",
    )
    return out


def solution(mesh):
    placed = (
        P("sp", "tp"),
        P("sp"),
        P("tp"),
        P("tp", None),
        P("sp", None),
        P(),
        P("sp", None),
        P("sp", None),
        P("sp", None, "tp"),
        P("sp", None, "tp"),
        P("sp", "tp", None),
        P(),
    )
    return jax.shard_map(
        shards, mesh=mesh, in_specs=placed, out_specs=P("sp", None), check_vma=False
    )
```

time: 341 us -> 166 us (0.49)
  waiting for transfers between devices: 202 us -> 80.7 us
  matrix products: 39.7 us -> 0 us
  blocking collectives: 31.5 us -> 0 us
  starting transfers between devices: 14.1 us -> 44.3 us
  Pallas kernels: 0 us -> 26.6 us
  other arithmetic: 23.1 us -> 0 us
  between operations: 13.4 us -> 0.17 us
  local copies, waits for them, and re-layouts: 16.5 us -> 13 us
    all_to_all x1 -> x0, waiting for transfers between devices: 93.2 us -> none  [shards(): lax.all_to_all(partial_value.reshape(senders, slot_count, width_all), 'sp...]
    ppermute x2 -> x33, waiting for transfers between devices: 0.01 us -> 80.7 us  [the longest x32 79.1 us: swap(): return lax.ppermute(value, axis, [(i, i ^ bits) for i in range(count)])]
    all_gather x2 -> x0, waiting for transfers between devices: 47.4 us -> none  [the longest x1 32.7 us: shards(): incoming = lax.all_gather(incoming, 'tp', axis=2, tiled=True)]
    dot_general x4 -> x0, matrix products: 39.7 us -> none  [the longest x1 20.6 us: shards(): jnp.dot(hidden, w_down[0], preferred_element_type=jnp.float32)]
    ppermute x2 -> x33, starting transfers between devices: 8.3 us -> 44.3 us  [the longest x32 39.3 us: swap(): return lax.ppermute(value, axis, [(i, i ^ bits) for i in range(count)])]
    psum x1 -> x0, waiting for transfers between devices: 34.6 us -> none  [shards(): routed = lax.psum(weighted.astype(jnp.bfloat16), 'tp').astype(jnp.float32)]
    all_to_all x1 -> x0, blocking collectives: 31.5 us -> none  [shards(): lax.all_to_all(outgoing, 'sp', split_axis=0, concat_axis=0, tiled=True)]
    pallas_call x0 -> x15, Pallas kernels: none -> 26.6 us  [call(): pl.pallas_call(body, out_shape=[jax.ShapeDtypeStruct(shape, kind) for sha...]
  transfers between devices with their start and end apart: 7 -> 33, of which waited for: 5 -> 18; matrix products, arithmetic and copies ran while one was open for 1% -> 0% of each run, Pallas kernels for 0% -> 13%
where the time goes in v1:
time: 166 us; the launch traced here: 165 us
  waiting for transfers between devices  80.7 us (49%)
  starting transfers between devices  44.3 us (27%)
  Pallas kernels  26.6 us (16%)
  local copies, waits for them, and re-layouts  13 us (8%)
    ppermute x32, waiting for transfers between devices, swap(): return lax.ppermute(value, axis, [(i, i ^ bits) for i in range(count)])  79.1 us
    ppermute x32, starting transfers between devices, swap(): return lax.ppermute(value, axis, [(i, i ^ bits) for i in range(count)])  39.3 us
    pallas_call x15, Pallas kernels, call(): pl.pallas_call(body, out_shape=[jax.ShapeDtypeStruct(shape, kind) for sha...  26.6 us
    unnamed x26, local copies, waits for them, and re-layouts  13 us
    ppermute x1, starting transfers between devices, shards(): pack = lax.ppermute(pack, 'sp', [(i, i + 1) for i in range(experts - 1)])  5 us
  transfers between devices with their start and end apart: 33, of which 18 were waited for; matrix products, arithmetic and copies ran while one was open for 0% of the time, Pallas kernels for 13%

profile of v1, /device:TPU:0, one launch (start us, length us, event | category | flops | bytes accessed | tf_op | source)
XLA Modules:
  0.0 164.8 jit_solution(11424567175371100934)
XLA Ops:
  0.0 0.9 copy-done.2
  1.0 0.7 copy-done.4
  1.6 5.0 %collective-permute-start = (bf16[32,512]{1,0:T(8,128)(2,1)S(1)}, bf16[32,512]{1,0:T(8,128)(2,1)S(1)}, u32[]{:S(2)}, u32[]{:S(2)}) collective-permute-start(bf16[32,512]{1,0:T(8,128)(2,1)S(1)} %tail.1), channel_id=1, source_target_pairs={{0,4},{4,8},{8,12},{12,16},{16,20},{20,24},{24,28},{1,5},{5,9},{9,... | collective-permute-start | bytes 98312 | tf_op jit(solution)/shard_map/ppermute | solution.py:276
  6.7 1.6 collective-permute-done.pack
  8.2 1.6 copy-done
  9.8 0.7 copy-done.5
  10.5 1.2 mix.1
  11.7 0.1 collective-permute-start.1
  11.8 1.9 %collective-permute-done.1.arrived = bf16[256,1024]{1,0:T(8,128)(2,1)S(1)} collective-permute-done((bf16[256,1024]{1,0:T(8,128)(2,1)S(1)}, bf16[256,1024]{1,0:T(8,128)(2,1)S(1)}, u32[]{:S(2)}, u32[]{:S(2)}) %collective-permute-start.1) | collective-permute-done | bytes 524320 | tf_op jit(solution)/shard_map/ppermute | solution.py:22
  13.7 0.1 split.1
  13.8 1.6 collective-permute-start.2
  15.4 6.8 %collective-permute-done.2.refs_1_ = bf16[256,512]{1,0:T(8,128)(2,1)S(1)} collective-permute-done((bf16[256,512]{1,0:T(8,128)(2,1)S(1)}, bf16[256,512]{1,0:T(8,128)(2,1)S(1)}, u32[]{:S(2)}, u32[]{:S(2)}) %collective-permute-start.2) | collective-permute-done | bytes 262176 | tf_op jit(solution)/shard_map/ppermute | solution.py:22
  22.2 1.2 copy-done.1
  23.4 0.3 stats.1
  23.7 0.0 collective-permute-start.3
  23.8 1.6 collective-permute-start.4
  25.4 0.3 collective-permute-start.5
  25.6 1.9 %collective-permute-done.4.refs_2_ = f32[8,256]{1,0:T(8,128)S(1)} collective-permute-done((f32[8,256]{1,0:T(8,128)S(1)}, f32[8,256]{1,0:T(8,128)S(1)}, u32[]{:S(2)}, u32[]{:S(2)}) %collective-permute-start.4) | collective-permute-done | bytes 8224 | tf_op jit(solution)/shard_map/ppermute | solution.py:22
  27.5 0.9 collective-permute-done.5.refs_3_
  28.4 0.7 dispatch.1
  29.1 4.4 %collective-permute-start.17 = (bf16[128,512]{1,0:T(8,128)(2,1)S(1)}, bf16[128,512]{1,0:T(8,128)(2,1)S(1)}, u32[]{:S(2)}, u32[]{:S(2)}) collective-permute-start(bf16[128,512]{1,0:T(8,128)(2,1)S(1)} %get-tuple-element.54), channel_id=1, source_target_pairs={{0,16},{4,20},{8,24},{12,28},{16,0},{20,4},{24,8},{28,12},{1,17},{... | collective-permute-start | bytes 393224 | tf_op jit(solution)/shard_map/ppermute | solution.py:22
  33.5 0.4 collective-permute-start.18
  33.9 3.6 %collective-permute-start.19 = (bf16[128,512]{1,0:T(8,128)(2,1)S(1)}, bf16[128,512]{1,0:T(8,128)(2,1)S(1)}, u32[]{:S(2)}, u32[]{:S(2)}) collective-permute-start(bf16[128,512]{1,0:T(8,128)(2,1)S(1)} %get-tuple-element.56), channel_id=1, source_target_pairs={{0,24},{4,28},{8,16},{12,20},{16,8},{20,12},{24,0},{28,4},{1,25},{... | collective-permute-start | bytes 393224 | tf_op jit(solution)/shard_map/ppermute | solution.py:22
  37.5 0.9 collective-permute-start.20
  38.4 10.7 %collective-permute-done.17.refs_0_ = bf16[128,512]{1,0:T(8,128)(2,1)S(1)} collective-permute-done((bf16[128,512]{1,0:T(8,128)(2,1)S(1)}, bf16[128,512]{1,0:T(8,128)(2,1)S(1)}, u32[]{:S(2)}, u32[]{:S(2)}) %collective-permute-start.17) | collective-permute-done | bytes 131104 | tf_op jit(solution)/shard_map/ppermute | solution.py:22
  49.1 3.2 %collective-permute-done.18.refs_1_ = bf16[128,512]{1,0:T(8,128)(2,1)S(1)} collective-permute-done((bf16[128,512]{1,0:T(8,128)(2,1)S(1)}, bf16[128,512]{1,0:T(8,128)(2,1)S(1)}, u32[]{:S(2)}, u32[]{:S(2)}) %collective-permute-start.18) | collective-permute-done | bytes 131104 | tf_op jit(solution)/shard_map/ppermute | solution.py:22
  52.3 0.7 collective-permute-start.21
  53.0 1.1 collective-permute-start.6
  54.1 5.6 %collective-permute-start.7 = (bf16[128,512]{1,0:T(8,128)(2,1)S(1)}, bf16[128,512]{1,0:T(8,128)(2,1)S(1)}, u32[]{:S(2)}, u32[]{:S(2)}) collective-permute-start(bf16[128,512]{1,0:T(8,128)(2,1)S(1)} %get-tuple-element.44), channel_id=1, source_target_pairs={{0,8},{4,12},{8,0},{12,4},{16,24},{20,28},{24,16},{28,20},{1,9},{5... | collective-permute-start | bytes 393224 | tf_op jit(solution)/shard_map/ppermute | solution.py:22
  59.7 0.2 collective-permute-start.8
  59.8 3.8 %collective-permute-done.7.refs_2_ = bf16[128,512]{1,0:T(8,128)(2,1)S(1)} collective-permute-done((bf16[128,512]{1,0:T(8,128)(2,1)S(1)}, bf16[128,512]{1,0:T(8,128)(2,1)S(1)}, u32[]{:S(2)}, u32[]{:S(2)}) %collective-permute-start.7) | collective-permute-done | bytes 131104 | tf_op jit(solution)/shard_map/ppermute | solution.py:22
  63.6 2.2 %collective-permute-done.8.refs_3_ = bf16[128,512]{1,0:T(8,128)(2,1)S(1)} collective-permute-done((bf16[128,512]{1,0:T(8,128)(2,1)S(1)}, bf16[128,512]{1,0:T(8,128)(2,1)S(1)}, u32[]{:S(2)}, u32[]{:S(2)}) %collective-permute-start.8) | collective-permute-done | bytes 131104 | tf_op jit(solution)/shard_map/ppermute | solution.py:22
  65.8 1.5 collective-permute-start.9
  67.4 0.5 collective-permute-start.23
  67.9 10.8 %collective-permute-done.9.refs_1_ = bf16[512,512]{1,0:T(8,128)(2,1)S(1)} collective-permute-done((bf16[512,512]{1,0:T(8,128)(2,1)S(1)}, bf16[512,512]{1,0:T(8,128)(2,1)S(1)}, u32[]{:S(2)}, u32[]{:S(2)}) %collective-permute-start.9) | collective-permute-done | bytes 524320 | tf_op jit(solution)/shard_map/ppermute | solution.py:22
  78.7 0.0 copy-start.6
  78.7 2.6 %copy-done.6 = bf16[1,2048,1408]{2,1,0:T(8,128)(2,1)S(1)} copy-done((bf16[1,2048,1408]{2,1,0:T(8,128)(2,1)S(1)}, bf16[1,2048,1408]{2,1,0:T(8,128)(2,1)}, u32[]{:S(2)}) %copy-start.6) | copy-done | bytes 5767192
  81.3 2.6 %copy-done.8 = bf16[1,2048,1408]{2,1,0:T(8,128)(2,1)S(1)} copy-done((bf16[1,2048,1408]{2,1,0:T(8,128)(2,1)S(1)}, bf16[1,2048,1408]{2,1,0:T(8,128)(2,1)}, u32[]{:S(2)}) %copy-start.8) | copy-done | bytes 5767192
  83.9 2.6 %copy-done.9 = bf16[1,1408,2048]{2,1,0:T(8,128)(2,1)S(1)} copy-done((bf16[1,1408,2048]{2,1,0:T(8,128)(2,1)S(1)}, bf16[1,1408,2048]{2,1,0:T(8,128)(2,1)}, u32[]{:S(2)}) %copy-start.9) | copy-done | bytes 5767192
  86.6 10.1 %expert.3 = (bf16[512,1024]{1,0:T(8,128)(2,1)S(1)}, bf16[512,1024]{1,0:T(8,128)(2,1)S(1)}) custom-call(bf16[512,512]{1,0:T(8,128)(2,1)S(1)} %stack.3.refs_0_, bf16[512,512]{1,0:T(8,128)(2,1)S(1)} %collective-permute-done.21.refs_1_, bf16[512,512]{1,0:T(8,128)(2,1)S(1)} %collective-permute-done.22.refs_2_, ...), custom_call_target="tpu_custom_call" | custom-call | flops 8858370048 | tf_op jit(solution)/shard_map/expert/pallas_call | solution.py:35
  96.7 0.6 collective-permute-start.24
  97.2 10.3 %expert.2 = (bf16[512,1024]{1,0:T(8,128)(2,1)S(1)}, bf16[512,1024]{1,0:T(8,128)(2,1)S(1)}) custom-call(bf16[512,512]{1,0:T(8,128)(2,1)S(1)} %stack.2.refs_0_, bf16[512,512]{1,0:T(8,128)(2,1)S(1)} %collective-permute-done.9.refs_1_, bf16[512,512]{1,0:T(8,128)(2,1)S(1)} %collective-permute-done.10.refs_2_, ...), custom_call_target="tpu_custom_call" | custom-call | flops 8858370048 | tf_op jit(solution)/shard_map/expert/pallas_call | solution.py:35
  107.6 0.1 collective-permute-start.12
  107.7 0.2 part.3
  107.9 1.6 collective-permute-start.25
  109.5 0.8 collective-permute-done.12.arrived
  110.3 0.2 part.2
  110.5 1.6 collective-permute-start.13
  112.1 10.7 %collective-permute-done.25.refs_1_ = bf16[512,512]{1,0:T(8,128)(2,1)S(1)} collective-permute-done((bf16[512,512]{1,0:T(8,128)(2,1)S(1)}, bf16[512,512]{1,0:T(8,128)(2,1)S(1)}, u32[]{:S(2)}, u32[]{:S(2)}) %collective-permute-start.25) | collective-permute-done | bytes 524320 | tf_op jit(solution)/shard_map/ppermute | solution.py:22
  122.8 0.1 homeward.3
  122.9 6.3 %collective-permute-start.26 = (bf16[128,512]{1,0:T(8,128)(2,1)S(1)}, bf16[128,512]{1,0:T(8,128)(2,1)S(1)}, u32[]{:S(2)}, u32[]{:S(2)}) collective-permute-start(bf16[128,512]{1,0:T(8,128)(2,1)S(1)} %get-tuple-element.62), channel_id=1, source_target_pairs={{0,16},{4,20},{8,24},{12,28},{16,0},{20,4},{24,8},{28,12},{1,17},{... | collective-permute-start | bytes 393224 | tf_op jit(solution)/shard_map/ppermute | solution.py:22
  129.2 0.9 collective-permute-start.27
  130.1 3.9 %collective-permute-start.29 = (bf16[128,512]{1,0:T(8,128)(2,1)S(1)}, bf16[128,512]{1,0:T(8,128)(2,1)S(1)}, u32[]{:S(2)}, u32[]{:S(2)}) collective-permute-start(bf16[128,512]{1,0:T(8,128)(2,1)S(1)} %get-tuple-element.65), channel_id=1, source_target_pairs={{0,28},{4,24},{8,20},{12,16},{16,12},{20,8},{24,4},{28,0},{1,29},{... | collective-permute-start | bytes 393224 | tf_op jit(solution)/shard_map/ppermute | solution.py:22
  134.0 0.1 homeward.2
  134.1 1.5 collective-permute-start.14
  135.6 7.9 %collective-permute-done.26.refs_4_ = bf16[128,512]{1,0:T(8,128)(2,1)S(1)} collective-permute-done((bf16[128,512]{1,0:T(8,128)(2,1)S(1)}, bf16[128,512]{1,0:T(8,128)(2,1)S(1)}, u32[]{:S(2)}, u32[]{:S(2)}) %collective-permute-start.26) | collective-permute-done | bytes 131104 | tf_op jit(solution)/shard_map/ppermute | solution.py:22
  143.5 3.0 %collective-permute-done.27.refs_5_ = bf16[128,512]{1,0:T(8,128)(2,1)S(1)} collective-permute-done((bf16[128,512]{1,0:T(8,128)(2,1)S(1)}, bf16[128,512]{1,0:T(8,128)(2,1)S(1)}, u32[]{:S(2)}, u32[]{:S(2)}) %collective-permute-start.27) | collective-permute-done | bytes 131104 | tf_op jit(solution)/shard_map/ppermute | solution.py:22
  146.5 2.3 %collective-permute-done.15.refs_2_ = bf16[128,512]{1,0:T(8,128)(2,1)S(1)} collective-permute-done((bf16[128,512]{1,0:T(8,128)(2,1)S(1)}, bf16[128,512]{1,0:T(8,128)(2,1)S(1)}, u32[]{:S(2)}, u32[]{:S(2)}) %collective-permute-start.15) | collective-permute-done | bytes 131104 | tf_op jit(solution)/shard_map/ppermute | solution.py:22
  148.9 3.9 %collective-permute-done.16.refs_3_ = bf16[128,512]{1,0:T(8,128)(2,1)S(1)} collective-permute-done((bf16[128,512]{1,0:T(8,128)(2,1)S(1)}, bf16[128,512]{1,0:T(8,128)(2,1)S(1)}, u32[]{:S(2)}, u32[]{:S(2)}) %collective-permute-start.16) | collective-permute-done | bytes 131104 | tf_op jit(solution)/shard_map/ppermute | solution.py:22
  152.7 1.5 combine.1.refs_0_
  154.2 0.6 collective-permute-start.30
  154.8 6.8 %collective-permute-done.30.refs_1_ = bf16[256,512]{1,0:T(8,128)(2,1)S(1)} collective-permute-done((bf16[256,512]{1,0:T(8,128)(2,1)S(1)}, bf16[256,512]{1,0:T(8,128)(2,1)S(1)}, u32[]{:S(2)}, u32[]{:S(2)}) %collective-permute-start.30) | collective-permute-done | bytes 262176 | tf_op jit(solution)/shard_map/ppermute | solution.py:22
  161.6 1.5 collective-permute-done.32.refs_3_
  163.1 1.7 %norm.1 = bf16[256,2048]{1,0:T(8,128)(2,1)} custom-call(bf16[256,512]{1,0:T(8,128)(2,1)S(1)} %combine.1.refs_0_, bf16[256,512]{1,0:T(8,128)(2,1)S(1)} %collective-permute-done.30.refs_1_, bf16[256,512]{1,0:T(8,128)(2,1)S(1)} %collective-permute-done.31.refs_2_, bf16[256,512]{1,0:T(8,128)(2,1)S(1)} %collective-permute-done.32.refs_3_, f32[1,2048]{1,0:T(1,128)S(1)} %bitcast.9), custom_call_target="tpu_custom_call" | custom-call | flops 1000000 | tf_op jit(solution)/shard_map/norm/pallas_call | solution.py:35
  (43 shorter events, 0.2 us)
Async XLA Ops:
  0.0 0.9 copy-start.2
  1.0 0.7 copy-start.4
  1.6 26.8 %copy-start.10 = (f32[2048]{0:T(1024)S(1)}, f32[2048]{0:T(1024)}, u32[]{:S(2)}) copy-start(f32[2048]{0:T(1024)} %param.17) | copy-start | bytes 24580
  1.6 26.8 %copy-start.11 = (s32[256,2]{0,1:T(2,128)S(1)}, s32[256,2]{0,1:T(2,128)}, u32[]{:S(2)}) copy-start(s32[256,2]{0,1:T(2,128)} %param.18) | copy-start | bytes 6148
  1.6 6.6 %collective-permute-start = (bf16[32,512]{1,0:T(8,128)(2,1)S(1)}, bf16[32,512]{1,0:T(8,128)(2,1)S(1)}, u32[]{:S(2)}, u32[]{:S(2)}) collective-permute-start(bf16[32,512]{1,0:T(8,128)(2,1)S(1)} %tail.1), channel_id=1, source_target_pairs={{0,4},{4,8},{8,12},{12,16},{16,20},{20,24},{24,28},{1,5},{5,9},{9,... | collective-permute-start | bytes 98312 | tf_op jit(solution)/shard_map/ppermute | solution.py:276
  8.2 1.6 copy-start
  9.8 0.7 copy-start.5
  11.7 2.0 %collective-permute-start.1 = (bf16[256,1024]{1,0:T(8,128)(2,1)S(1)}, bf16[256,1024]{1,0:T(8,128)(2,1)S(1)}, u32[]{:S(2)}, u32[]{:S(2)}) collective-permute-start(bf16[256,1024]{1,0:T(8,128)(2,1)S(1)} %get-tuple-element.37), channel_id=1, source_target_pairs={{0,1},{1,0},{2,3},{3,2},{4,5},{5,4},{6,7},{7,6},{8,9},{9,8},{10,11... | collective-permute-start | bytes 1572872 | tf_op jit(solution)/shard_map/ppermute | solution.py:22
  13.8 8.4 %collective-permute-start.2 = (bf16[256,512]{1,0:T(8,128)(2,1)S(1)}, bf16[256,512]{1,0:T(8,128)(2,1)S(1)}, u32[]{:S(2)}, u32[]{:S(2)}) collective-permute-start(bf16[256,512]{1,0:T(8,128)(2,1)S(1)} %get-tuple-element.39), channel_id=1, source_target_pairs={{0,2},{1,3},{2,0},{3,1},{4,6},{5,7},{6,4},{7,5},{8,10},{9,11},{10,... | collective-permute-start | bytes 786440 | tf_op jit(solution)/shard_map/ppermute | solution.py:22
  22.2 1.2 copy-start.1
  23.7 1.9 %collective-permute-start.3 = (f32[8,256]{1,0:T(8,128)S(1)}, f32[8,256]{1,0:T(8,128)S(1)}, u32[]{:S(2)}, u32[]{:S(2)}) collective-permute-start(f32[8,256]{1,0:T(8,128)S(1)} %get-tuple-element.40.refs_0_), channel_id=1, source_target_pairs={{0,1},{1,0},{2,3},{3,2},{4,5},{5,4},{6,7},{7,6},{8,9},{9,8},{10,11... | collective-permute-start | bytes 24584 | tf_op jit(solution)/shard_map/ppermute | solution.py:22
  23.8 3.7 %collective-permute-start.4 = (f32[8,256]{1,0:T(8,128)S(1)}, f32[8,256]{1,0:T(8,128)S(1)}, u32[]{:S(2)}, u32[]{:S(2)}) collective-permute-start(f32[8,256]{1,0:T(8,128)S(1)} %get-tuple-element.40.refs_0_), channel_id=1, source_target_pairs={{0,2},{1,3},{2,0},{3,1},{4,6},{5,7},{6,4},{7,5},{8,10},{9,11},{10,... | collective-permute-start | bytes 24584 | tf_op jit(solution)/shard_map/ppermute | solution.py:22
  25.4 3.1 %collective-permute-start.5 = (f32[8,256]{1,0:T(8,128)S(1)}, f32[8,256]{1,0:T(8,128)S(1)}, u32[]{:S(2)}, u32[]{:S(2)}) collective-permute-start(f32[8,256]{1,0:T(8,128)S(1)} %get-tuple-element.40.refs_0_), channel_id=1, source_target_pairs={{0,3},{1,2},{2,1},{3,0},{4,7},{5,6},{6,5},{7,4},{8,11},{9,10},{10,... | collective-permute-start | bytes 24584 | tf_op jit(solution)/shard_map/ppermute | solution.py:22
  29.1 20.0 %collective-permute-start.17 = (bf16[128,512]{1,0:T(8,128)(2,1)S(1)}, bf16[128,512]{1,0:T(8,128)(2,1)S(1)}, u32[]{:S(2)}, u32[]{:S(2)}) collective-permute-start(bf16[128,512]{1,0:T(8,128)(2,1)S(1)} %get-tuple-element.54), channel_id=1, source_target_pairs={{0,16},{4,20},{8,24},{12,28},{16,0},{20,4},{24,8},{28,12},{1,17},{... | collective-permute-start | bytes 393224 | tf_op jit(solution)/shard_map/ppermute | solution.py:22
  33.5 18.7 %collective-permute-start.18 = (bf16[128,512]{1,0:T(8,128)(2,1)S(1)}, bf16[128,512]{1,0:T(8,128)(2,1)S(1)}, u32[]{:S(2)}, u32[]{:S(2)}) collective-permute-start(bf16[128,512]{1,0:T(8,128)(2,1)S(1)} %get-tuple-element.55), channel_id=1, source_target_pairs={{0,20},{4,16},{8,28},{12,24},{16,4},{20,0},{24,12},{28,8},{1,21},{... | collective-permute-start | bytes 393224 | tf_op jit(solution)/shard_map/ppermute | solution.py:22
  33.9 18.4 %collective-permute-start.19 = (bf16[128,512]{1,0:T(8,128)(2,1)S(1)}, bf16[128,512]{1,0:T(8,128)(2,1)S(1)}, u32[]{:S(2)}, u32[]{:S(2)}) collective-permute-start(bf16[128,512]{1,0:T(8,128)(2,1)S(1)} %get-tuple-element.56), channel_id=1, source_target_pairs={{0,24},{4,28},{8,16},{12,20},{16,8},{20,12},{24,0},{28,4},{1,25},{... | collective-permute-start | bytes 393224 | tf_op jit(solution)/shard_map/ppermute | solution.py:22
  37.5 14.8 %collective-permute-start.20 = (bf16[128,512]{1,0:T(8,128)(2,1)S(1)}, bf16[128,512]{1,0:T(8,128)(2,1)S(1)}, u32[]{:S(2)}, u32[]{:S(2)}) collective-permute-start(bf16[128,512]{1,0:T(8,128)(2,1)S(1)} %get-tuple-element.57), channel_id=1, source_target_pairs={{0,28},{4,24},{8,20},{12,16},{16,12},{20,8},{24,4},{28,0},{1,29},{... | collective-permute-start | bytes 393224 | tf_op jit(solution)/shard_map/ppermute | solution.py:22
  52.3 15.1 %collective-permute-start.21 = (bf16[512,512]{1,0:T(8,128)(2,1)S(1)}, bf16[512,512]{1,0:T(8,128)(2,1)S(1)}, u32[]{:S(2)}, u32[]{:S(2)}) collective-permute-start(bf16[512,512]{1,0:T(8,128)(2,1)S(1)} %stack.3.refs_0_), channel_id=1, source_target_pairs={{0,2},{1,3},{2,0},{3,1},{4,6},{5,7},{6,4},{7,5},{8,10},{9,11},{10,... | collective-permute-start | bytes 1572872 | tf_op jit(solution)/shard_map/ppermute | solution.py:22
  53.0 6.9 %collective-permute-start.6 = (bf16[128,512]{1,0:T(8,128)(2,1)S(1)}, bf16[128,512]{1,0:T(8,128)(2,1)S(1)}, u32[]{:S(2)}, u32[]{:S(2)}) collective-permute-start(bf16[128,512]{1,0:T(8,128)(2,1)S(1)} %get-tuple-element.43), channel_id=1, source_target_pairs={{0,4},{4,0},{8,12},{12,8},{16,20},{20,16},{24,28},{28,24},{1,5},{5... | collective-permute-start | bytes 393224 | tf_op jit(solution)/shard_map/ppermute | solution.py:22
  54.1 9.5 %collective-permute-start.7 = (bf16[128,512]{1,0:T(8,128)(2,1)S(1)}, bf16[128,512]{1,0:T(8,128)(2,1)S(1)}, u32[]{:S(2)}, u32[]{:S(2)}) collective-permute-start(bf16[128,512]{1,0:T(8,128)(2,1)S(1)} %get-tuple-element.44), channel_id=1, source_target_pairs={{0,8},{4,12},{8,0},{12,4},{16,24},{20,28},{24,16},{28,20},{1,9},{5... | collective-permute-start | bytes 393224 | tf_op jit(solution)/shard_map/ppermute | solution.py:22
  59.7 6.1 %collective-permute-start.8 = (bf16[128,512]{1,0:T(8,128)(2,1)S(1)}, bf16[128,512]{1,0:T(8,128)(2,1)S(1)}, u32[]{:S(2)}, u32[]{:S(2)}) collective-permute-start(bf16[128,512]{1,0:T(8,128)(2,1)S(1)} %get-tuple-element.45), channel_id=1, source_target_pairs={{0,12},{4,8},{8,4},{12,0},{16,28},{20,24},{24,20},{28,16},{1,13},{... | collective-permute-start | bytes 393224 | tf_op jit(solution)/shard_map/ppermute | solution.py:22
  65.8 12.8 %collective-permute-start.9 = (bf16[512,512]{1,0:T(8,128)(2,1)S(1)}, bf16[512,512]{1,0:T(8,128)(2,1)S(1)}, u32[]{:S(2)}, u32[]{:S(2)}) collective-permute-start(bf16[512,512]{1,0:T(8,128)(2,1)S(1)} %stack.2.refs_0_), channel_id=1, source_target_pairs={{0,2},{1,3},{2,0},{3,1},{4,6},{5,7},{6,4},{7,5},{8,10},{9,11},{10,... | collective-permute-start | bytes 1572872 | tf_op jit(solution)/shard_map/ppermute | solution.py:22
  67.4 11.3 %collective-permute-start.22 = (bf16[512,512]{1,0:T(8,128)(2,1)S(1)}, bf16[512,512]{1,0:T(8,128)(2,1)S(1)}, u32[]{:S(2)}, u32[]{:S(2)}) collective-permute-start(bf16[512,512]{1,0:T(8,128)(2,1)S(1)} %stack.3.refs_0_), channel_id=1, source_target_pairs={{0,1},{1,0},{2,3},{3,2},{4,5},{5,4},{6,7},{7,6},{8,9},{9,8},{10,11... | collective-permute-start | bytes 1572872 | tf_op jit(solution)/shard_map/ppermute | solution.py:22
  67.4 11.3 %collective-permute-start.23 = (bf16[512,512]{1,0:T(8,128)(2,1)S(1)}, bf16[512,512]{1,0:T(8,128)(2,1)S(1)}, u32[]{:S(2)}, u32[]{:S(2)}) collective-permute-start(bf16[512,512]{1,0:T(8,128)(2,1)S(1)} %collective-permute-done.21.refs_1_), channel_id=1, source_target_pairs={{0,1},{1,0},{2,3},{3,2},{4,5},{5,4},{6,7},{7,6},{8,9},{9,8},{10,11... | collective-permute-start | bytes 1572872 | tf_op jit(solution)/shard_map/ppermute | solution.py:22
  67.9 29.4 %collective-permute-start.10 = (bf16[512,512]{1,0:T(8,128)(2,1)S(1)}, bf16[512,512]{1,0:T(8,128)(2,1)S(1)}, u32[]{:S(2)}, u32[]{:S(2)}) collective-permute-start(bf16[512,512]{1,0:T(8,128)(2,1)S(1)} %stack.2.refs_0_), channel_id=1, source_target_pairs={{0,1},{1,0},{2,3},{3,2},{4,5},{5,4},{6,7},{7,6},{8,9},{9,8},{10,11... | collective-permute-start | bytes 1572872 | tf_op jit(solution)/shard_map/ppermute | solution.py:22
  78.6 18.6 %collective-permute-start.11 = (bf16[512,512]{1,0:T(8,128)(2,1)S(1)}, bf16[512,512]{1,0:T(8,128)(2,1)S(1)}, u32[]{:S(2)}, u32[]{:S(2)}) collective-permute-start(bf16[512,512]{1,0:T(8,128)(2,1)S(1)} %collective-permute-done.9.refs_1_), channel_id=1, source_target_pairs={{0,1},{1,0},{2,3},{3,2},{4,5},{5,4},{6,7},{7,6},{8,9},{9,8},{10,11... | collective-permute-start | bytes 1572872 | tf_op jit(solution)/shard_map/ppermute | solution.py:22
  78.7 2.6 %copy-start.6 = (bf16[1,2048,1408]{2,1,0:T(8,128)(2,1)S(1)}, bf16[1,2048,1408]{2,1,0:T(8,128)(2,1)}, u32[]{:S(2)}) copy-start(bf16[1,2048,1408]{2,1,0:T(8,128)(2,1)} %param.20) | copy-start | bytes 17301508
  81.3 2.6 %copy-start.8 = (bf16[1,2048,1408]{2,1,0:T(8,128)(2,1)S(1)}, bf16[1,2048,1408]{2,1,0:T(8,128)(2,1)}, u32[]{:S(2)}) copy-start(bf16[1,2048,1408]{2,1,0:T(8,128)(2,1)} %param.21) | copy-start | bytes 17301508
  83.9 2.6 %copy-start.9 = (bf16[1,1408,2048]{2,1,0:T(8,128)(2,1)S(1)}, bf16[1,1408,2048]{2,1,0:T(8,128)(2,1)}, u32[]{:S(2)}) copy-start(bf16[1,1408,2048]{2,1,0:T(8,128)(2,1)} %param.22) | copy-start | bytes 17301508
  86.6 10.7 %copy-start.7 = (bf16[1,2048,1408]{2,1,0:T(8,128)(2,1)S(1)}, bf16[1,2048,1408]{2,1,0:T(8,128)(2,1)}, u32[]{:S(2)}) copy-start(bf16[1,2048,1408]{2,1,0:T(8,128)(2,1)} %param.20) | copy-start | bytes 17301508
  96.7 11.0 %collective-permute-start.24 = (bf16[512,1024]{1,0:T(8,128)(2,1)S(1)}, bf16[512,1024]{1,0:T(8,128)(2,1)S(1)}, u32[]{:S(2)}, u32[]{:S(2)}) collective-permute-start(bf16[512,1024]{1,0:T(8,128)(2,1)S(1)} %get-tuple-element.59), channel_id=1, source_target_pairs={{0,1},{1,0},{2,3},{3,2},{4,5},{5,4},{6,7},{7,6},{8,9},{9,8},{10,11... | collective-permute-start | bytes 3145736 | tf_op jit(solution)/shard_map/ppermute | solution.py:22
  107.5 45.2 %copy-start.12 = (f32[256,2]{0,1:T(2,128)S(1)}, f32[256,2]{0,1:T(2,128)}, u32[]{:S(2)}) copy-start(f32[256,2]{0,1:T(2,128)} %param.19) | copy-start | bytes 6148
  107.6 55.6 %copy-start.3 = (f32[2048]{0:T(1024)S(1)}, f32[2048]{0:T(1024)}, u32[]{:S(2)}) copy-start(f32[2048]{0:T(1024)} %param.23) | copy-start | bytes 24580
  107.6 2.7 %collective-permute-start.12 = (bf16[512,1024]{1,0:T(8,128)(2,1)S(1)}, bf16[512,1024]{1,0:T(8,128)(2,1)S(1)}, u32[]{:S(2)}, u32[]{:S(2)}) collective-permute-start(bf16[512,1024]{1,0:T(8,128)(2,1)S(1)} %get-tuple-element.47), channel_id=1, source_target_pairs={{0,1},{1,0},{2,3},{3,2},{4,5},{5,4},{6,7},{7,6},{8,9},{9,8},{10,11... | collective-permute-start | bytes 3145736 | tf_op jit(solution)/shard_map/ppermute | solution.py:22
  107.9 14.9 %collective-permute-start.25 = (bf16[512,512]{1,0:T(8,128)(2,1)S(1)}, bf16[512,512]{1,0:T(8,128)(2,1)S(1)}, u32[]{:S(2)}, u32[]{:S(2)}) collective-permute-start(bf16[512,512]{1,0:T(8,128)(2,1)S(1)} %get-tuple-element.61), channel_id=1, source_target_pairs={{0,2},{1,3},{2,0},{3,1},{4,6},{5,7},{6,4},{7,5},{8,10},{9,11},{10,... | collective-permute-start | bytes 1572872 | tf_op jit(solution)/shard_map/ppermute | solution.py:22
  110.5 23.5 %collective-permute-start.13 = (bf16[512,512]{1,0:T(8,128)(2,1)S(1)}, bf16[512,512]{1,0:T(8,128)(2,1)S(1)}, u32[]{:S(2)}, u32[]{:S(2)}) collective-permute-start(bf16[512,512]{1,0:T(8,128)(2,1)S(1)} %get-tuple-element.49), channel_id=1, source_target_pairs={{0,2},{1,3},{2,0},{3,1},{4,6},{5,7},{6,4},{7,5},{8,10},{9,11},{10,... | collective-permute-start | bytes 1572872 | tf_op jit(solution)/shard_map/ppermute | solution.py:22
  122.9 20.6 %collective-permute-start.26 = (bf16[128,512]{1,0:T(8,128)(2,1)S(1)}, bf16[128,512]{1,0:T(8,128)(2,1)S(1)}, u32[]{:S(2)}, u32[]{:S(2)}) collective-permute-start(bf16[128,512]{1,0:T(8,128)(2,1)S(1)} %get-tuple-element.62), channel_id=1, source_target_pairs={{0,16},{4,20},{8,24},{12,28},{16,0},{20,4},{24,8},{28,12},{1,17},{... | collective-permute-start | bytes 393224 | tf_op jit(solution)/shard_map/ppermute | solution.py:22
  129.2 17.3 %collective-permute-start.27 = (bf16[128,512]{1,0:T(8,128)(2,1)S(1)}, bf16[128,512]{1,0:T(8,128)(2,1)S(1)}, u32[]{:S(2)}, u32[]{:S(2)}) collective-permute-start(bf16[128,512]{1,0:T(8,128)(2,1)S(1)} %get-tuple-element.63), channel_id=1, source_target_pairs={{0,20},{4,16},{8,28},{12,24},{16,4},{20,0},{24,12},{28,8},{1,21},{... | collective-permute-start | bytes 393224 | tf_op jit(solution)/shard_map/ppermute | solution.py:22
  130.1 16.4 %collective-permute-start.28 = (bf16[128,512]{1,0:T(8,128)(2,1)S(1)}, bf16[128,512]{1,0:T(8,128)(2,1)S(1)}, u32[]{:S(2)}, u32[]{:S(2)}) collective-permute-start(bf16[128,512]{1,0:T(8,128)(2,1)S(1)} %get-tuple-element.64), channel_id=1, source_target_pairs={{0,24},{4,28},{8,16},{12,20},{16,8},{20,12},{24,0},{28,4},{1,25},{... | collective-permute-start | bytes 393224 | tf_op jit(solution)/shard_map/ppermute | solution.py:22
  130.1 16.4 %collective-permute-start.29 = (bf16[128,512]{1,0:T(8,128)(2,1)S(1)}, bf16[128,512]{1,0:T(8,128)(2,1)S(1)}, u32[]{:S(2)}, u32[]{:S(2)}) collective-permute-start(bf16[128,512]{1,0:T(8,128)(2,1)S(1)} %get-tuple-element.65), channel_id=1, source_target_pairs={{0,28},{4,24},{8,20},{12,16},{16,12},{20,8},{24,4},{28,0},{1,29},{... | collective-permute-start | bytes 393224 | tf_op jit(solution)/shard_map/ppermute | solution.py:22
  134.1 12.4 %collective-permute-start.14 = (bf16[128,512]{1,0:T(8,128)(2,1)S(1)}, bf16[128,512]{1,0:T(8,128)(2,1)S(1)}, u32[]{:S(2)}, u32[]{:S(2)}) collective-permute-start(bf16[128,512]{1,0:T(8,128)(2,1)S(1)} %get-tuple-element.51), channel_id=1, source_target_pairs={{0,4},{4,0},{8,12},{12,8},{16,20},{20,16},{24,28},{28,24},{1,5},{5... | collective-permute-start | bytes 393224 | tf_op jit(solution)/shard_map/ppermute | solution.py:22
  143.5 5.4 %collective-permute-start.15 = (bf16[128,512]{1,0:T(8,128)(2,1)S(1)}, bf16[128,512]{1,0:T(8,128)(2,1)S(1)}, u32[]{:S(2)}, u32[]{:S(2)}) collective-permute-start(bf16[128,512]{1,0:T(8,128)(2,1)S(1)} %get-tuple-element.52), channel_id=1, source_target_pairs={{0,8},{4,12},{8,0},{12,4},{16,24},{20,28},{24,16},{28,20},{1,9},{5... | collective-permute-start | bytes 393224 | tf_op jit(solution)/shard_map/ppermute | solution.py:22
  146.5 6.2 %collective-permute-start.16 = (bf16[128,512]{1,0:T(8,128)(2,1)S(1)}, bf16[128,512]{1,0:T(8,128)(2,1)S(1)}, u32[]{:S(2)}, u32[]{:S(2)}) collective-permute-start(bf16[128,512]{1,0:T(8,128)(2,1)S(1)} %get-tuple-element.53), channel_id=1, source_target_pairs={{0,12},{4,8},{8,4},{12,0},{16,28},{20,24},{24,20},{28,16},{1,13},{... | collective-permute-start | bytes 393224 | tf_op jit(solution)/shard_map/ppermute | solution.py:22
  154.2 7.3 %collective-permute-start.30 = (bf16[256,512]{1,0:T(8,128)(2,1)S(1)}, bf16[256,512]{1,0:T(8,128)(2,1)S(1)}, u32[]{:S(2)}, u32[]{:S(2)}) collective-permute-start(bf16[256,512]{1,0:T(8,128)(2,1)S(1)} %combine.1.refs_0_), channel_id=1, source_target_pairs={{0,2},{1,3},{2,0},{3,1},{4,6},{5,7},{6,4},{7,5},{8,10},{9,11},{10,... | collective-permute-start | bytes 786440 | tf_op jit(solution)/shard_map/ppermute | solution.py:22
  154.8 6.8 %collective-permute-start.31 = (bf16[256,512]{1,0:T(8,128)(2,1)S(1)}, bf16[256,512]{1,0:T(8,128)(2,1)S(1)}, u32[]{:S(2)}, u32[]{:S(2)}) collective-permute-start(bf16[256,512]{1,0:T(8,128)(2,1)S(1)} %combine.1.refs_0_), channel_id=1, source_target_pairs={{0,1},{1,0},{2,3},{3,2},{4,5},{5,4},{6,7},{7,6},{8,9},{9,8},{10,11... | collective-permute-start | bytes 786440 | tf_op jit(solution)/shard_map/ppermute | solution.py:22
  161.6 1.5 collective-permute-start.32

commit v2 on v1

--- a/solution.py
+++ b/solution.py
@@ -7,12 +7,13 @@
 from jax.experimental.pallas import tpu as pltpu
 from jax.sharding import PartitionSpec as P
 
+
 alpha_res = 1.4142135623730951
 norm_eps = 1e-05
 reach = 16
 lanes = 128
 f32, bf16 = jnp.float32, jnp.bfloat16
-MIB = 2**20
+MIB, GIGA = 2**20, 10**9
 
 
 def swap(value, axis, bits):
@@ -30,7 +31,7 @@
     return jnp.dot(a, b, preferred_element_type=f32)
 
 
-def call(body, outs, operands, scratch=(), flops=1_000_000, vmem=16, name=None):
+def call(body, outs, operands, scratch=(), flops=3 * GIGA, vmem=16):
     whole = pl.BlockSpec(memory_space=pltpu.VMEM)
     return pl.pallas_call(
         body,
@@ -40,7 +41,6 @@
         scratch_shapes=list(scratch),
         compiler_params=pltpu.CompilerParams(vmem_limit_bytes=vmem * MIB),
         cost_estimate=pl.CostEstimate(flops=flops, bytes_accessed=0, transcendentals=0),
-        name=name,
     )(*operands)
 
 
@@ -60,7 +60,7 @@
 def tail_body(x, docs, pack):
     rows = x.shape[0]
     pack[0:reach, :] = x[rows - reach :, :]
-    pack[reach:, :] = jnp.zeros_like(pack[reach:, :])
+    pack[reach:, :] = jnp.zeros((reach, x.shape[1]), bf16)
     pack[reach:, 0:lanes] = jnp.broadcast_to(
         docs[:, rows - lanes :].astype(f32), (reach, lanes)
     ).astype(bf16)
@@ -112,8 +112,8 @@
 
 def stats_body(parts, *refs):
     own, arrived, residual, z_out, stats = refs[0], refs[1:parts], refs[parts], refs[-2], refs[-1]
+    width = own.shape[1]
     core, y, y_parts = place()
-    width = own.shape[1]
     z = alpha_res * residual[:, columns((core * y_parts + y) * width, width)].astype(f32)
     shares = own[...]
     for ref in arrived:
@@ -245,8 +245,11 @@
 
 
 def over_tp(value, y_parts):
-    mine = [swap(value, "tp", bits << 1) for bits in range(y_parts)]
+    mine = [swap(value, "tp", i << 1) for i in range(y_parts)]
     return mine + [swap(part, "tp", 1) for part in mine]
+
+
+chunks = 4
 
 
 def shards(
@@ -269,48 +272,45 @@
     y_parts = devices // 2
     half, part = features // 2, features // devices
     capacity = 4 * tokens // experts
+    ids, pair_weight = expert_ids.T, expert_weight.T
+
     docs = doc_ids.reshape(1, tokens)
-    ids, pair_weight = expert_ids.T, expert_weight.T
-
-    (pack,) = call(tail_body, [((2 * reach, cols), bf16)], (mixer_in, docs), name="tail")
+    (pack,) = call(tail_body, [((2 * reach, cols), bf16)], (mixer_in, docs), flops=8 * GIGA)
     pack = lax.ppermute(pack, "sp", [(i, i + 1) for i in range(experts - 1)])
     keep, send = call(
         mix_body,
         [((tokens, half), f32), ((tokens, half), bf16)],
         (mixer_in, pack, docs, mix_scale.reshape(1, cols), out_proj),
-        flops=2 * tokens * cols * features,
-        name="mix",
+        flops=2 * GIGA,
     )
     arrived = swap(send, "tp", 1)
     own, *sends = call(
         split_body,
         [((tokens, part), f32)] + [((tokens, part), bf16)] * (y_parts - 1),
         (keep, arrived),
-        name="split",
-    )
-    shares = [swap(v, "tp", (i + 1) << 1) for i, v in enumerate(sends)]
+        flops=10 * GIGA,
+    )
+    shares = [swap(v, "tp", i << 1) for i, v in enumerate(sends, 1)]
     z, stats = call(
         functools.partial(stats_body, y_parts),
         [((tokens, part), f32), ((8, tokens), f32)],
         (own, *shares, residual),
-        name="stats",
-    )
-    every = [swap(stats, "tp", bits) for bits in range(devices)]
+        flops=6 * GIGA,
+    )
+    every = [swap(stats, "tp", i) for i in range(devices)]
     normed, *outgoing = call(
         functools.partial(dispatch_body, devices, experts),
         [((tokens, part), bf16)] + [((capacity, part), bf16)] * experts,
         (*every, z, mix_gain.reshape(1, features), ids),
-        flops=2 * tokens * tokens * part * 4,
-        name="dispatch",
-    )
-    incoming = [swap(v, "sp", bits) for bits, v in enumerate(outgoing)]
-    group = experts // 2
+        flops=10 * GIGA,
+    )
+    incoming = [swap(v, "sp", i) for i, v in enumerate(outgoing)]
+    group = experts // chunks
     rows = group * capacity
     returned = []
-    for first in range(0, experts, group):
-        (stacked,) = call(
-            stack_body, [((rows, part), bf16)], incoming[first : first + group], name="stack"
-        )
+    for at in range(chunks):
+        first = at * group
+        (stacked,) = call(stack_body, [((rows, part), bf16)], incoming[first : first + group])
         pieces = over_tp(stacked, y_parts)
         send, keep = call(
             functools.partial(expert_body, len(pieces)),
@@ -321,37 +321,28 @@
                 pltpu.VMEM((rows, w_gate.shape[2]), bf16),
             ],
             flops=6 * rows * features * w_gate.shape[2],
-            vmem=24,
-            name="expert",
+            vmem=16,
         )
         arrived = swap(send, "tp", 1)
-        own, *sends = call(
-            split_body,
-            [((rows, part), bf16)] * y_parts,
-            (keep, arrived),
-            name="part",
-        )
-        shares = [swap(v, "tp", (i + 1) << 1) for i, v in enumerate(sends)]
+        own, *sends = call(split_body, [((rows, part), bf16)] * y_parts, (keep, arrived))
+        shares = [swap(v, "tp", i << 1) for i, v in enumerate(sends, 1)]
         homeward = call(
             functools.partial(homeward_body, y_parts),
             [((capacity, part), bf16)] * group,
             (own, *shares),
-            name="homeward",
         )
-        returned += [swap(v, "sp", first + i) for i, v in enumerate(homeward)]
+        returned += [swap(v, "sp", i) for i, v in enumerate(homeward, first)]
     (z,) = call(
         functools.partial(combine_body, experts),
         [((tokens, part), bf16)],
         (*returned, ids, pair_weight, normed),
         flops=4 * tokens * experts * capacity * part,
-        name="combine",
     )
     (out,) = call(
         norm_body,
         [((tokens, features), bf16)],
         (*over_tp(z, y_parts), out_gain.reshape(1, features)),
         scratch=[pltpu.VMEM((tokens, features), bf16)],
-        name="norm",
     )
     return out
 

time: 166 us -> 143 us (0.86)
  waiting for transfers between devices: 80.7 us -> 64.6 us
  local copies, waits for them, and re-layouts: 13 us -> 1.69 us
  starting transfers between devices: 44.3 us -> 49.6 us
    ppermute x32 -> x42, waiting for transfers between devices: 79.1 us -> 63 us  [swap(): return lax.ppermute(value, axis, [(i, i ^ bits) for i in range(count)])]
    unnamed x26 -> x30, local copies, waits for them, and re-layouts: 13 us -> 1.69 us
    ppermute x32 -> x42, starting transfers between devices: 39.3 us -> 44.6 us  [swap(): return lax.ppermute(value, axis, [(i, i ^ bits) for i in range(count)])]
    pallas_call x15 -> x23, Pallas kernels: 26.6 us -> 26.9 us  [call(): pl.pallas_call(body, out_shape=[jax.ShapeDtypeStruct(shape, kind) for sha...]
  transfers between devices with their start and end apart: 33 -> 43, of which waited for: 18 -> 22; matrix products, arithmetic and copies ran while one was open for 0% -> 0% of each run, Pallas kernels for 13% -> 15%
where the time goes in v2:
time: 143 us
  waiting for transfers between devices  64.6 us (45%)
  starting transfers between devices  49.6 us (35%)
  Pallas kernels  26.9 us (19%)
  local copies, waits for them, and re-layouts  1.69 us (1%)
    ppermute x42, waiting for transfers between devices, swap(): return lax.ppermute(value, axis, [(i, i ^ bits) for i in range(count)])  63 us
    ppermute x42, starting transfers between devices, swap(): return lax.ppermute(value, axis, [(i, i ^ bits) for i in range(count)])  44.6 us
    pallas_call x23, Pallas kernels, call(): pl.pallas_call(body, out_shape=[jax.ShapeDtypeStruct(shape, kind) for sha...  26.9 us
    ppermute x1, starting transfers between devices, shards(): pack = lax.ppermute(pack, 'sp', [(i, i + 1) for i in range(experts - 1)])  5 us
  transfers between devices with their start and end apart: 43, of which 22 were waited for; matrix products, arithmetic and copies ran while one was open for 0% of the time, Pallas kernels for 15%

profile of v2, /device:TPU:0, one launch (start us, length us, event | category | flops | bytes accessed | tf_op | source)
XLA Modules:
  0.0 143.1 jit_solution(5264814646106204969)
XLA Ops:
  0.0 0.9 copy-done.2
  1.0 0.7 copy-done.8
  1.6 5.0 %collective-permute-start = (bf16[32,512]{1,0:T(8,128)(2,1)S(1)}, bf16[32,512]{1,0:T(8,128)(2,1)S(1)}, u32[]{:S(2)}, u32[]{:S(2)}) collective-permute-start(bf16[32,512]{1,0:T(8,128)(2,1)S(1)} %shard_map.118), channel_id=1, source_target_pairs={{0,4},{4,8},{8,12},{12,16},{16,20},{20,24},{24,28},{1,5},{5,9},{9,... | collective-permute-start | bytes 98312 | tf_op jit(solution)/shard_map/ppermute | solution.py:279
  6.7 1.6 %collective-permute-done.pack = bf16[32,512]{1,0:T(8,128)(2,1)S(1)} collective-permute-done((bf16[32,512]{1,0:T(8,128)(2,1)S(1)}, bf16[32,512]{1,0:T(8,128)(2,1)S(1)}, u32[]{:S(2)}, u32[]{:S(2)}) %collective-permute-start) | collective-permute-done | bytes 32800 | tf_op jit(solution)/shard_map/ppermute | solution.py:279
  8.2 1.2 shard_map.119
  9.5 1.9 %collective-permute-done.1.arrived = bf16[256,1024]{1,0:T(8,128)(2,1)S(1)} collective-permute-done((bf16[256,1024]{1,0:T(8,128)(2,1)S(1)}, bf16[256,1024]{1,0:T(8,128)(2,1)S(1)}, u32[]{:S(2)}, u32[]{:S(2)}) %collective-permute-start.1) | collective-permute-done | bytes 524320 | tf_op jit(solution)/shard_map/ppermute | solution.py:23
  11.5 1.6 %collective-permute-start.2 = (bf16[256,512]{1,0:T(8,128)(2,1)S(1)}, bf16[256,512]{1,0:T(8,128)(2,1)S(1)}, u32[]{:S(2)}, u32[]{:S(2)}) collective-permute-start(bf16[256,512]{1,0:T(8,128)(2,1)S(1)} %get-tuple-element.47), channel_id=1, source_target_pairs={{0,2},{1,3},{2,0},{3,1},{4,6},{5,7},{6,4},{7,5},{8,10},{9,11},{10,... | collective-permute-start | bytes 786440 | tf_op jit(solution)/shard_map/ppermute | solution.py:23
  13.1 6.8 %collective-permute-done.2.refs_1_ = bf16[256,512]{1,0:T(8,128)(2,1)S(1)} collective-permute-done((bf16[256,512]{1,0:T(8,128)(2,1)S(1)}, bf16[256,512]{1,0:T(8,128)(2,1)S(1)}, u32[]{:S(2)}, u32[]{:S(2)}) %collective-permute-start.2) | collective-permute-done | bytes 262176 | tf_op jit(solution)/shard_map/ppermute | solution.py:23
  19.9 0.3 shard_map.121
  20.3 1.6 %collective-permute-start.4 = (f32[8,256]{1,0:T(8,128)S(1)}, f32[8,256]{1,0:T(8,128)S(1)}, u32[]{:S(2)}, u32[]{:S(2)}) collective-permute-start(f32[8,256]{1,0:T(8,128)S(1)} %get-tuple-element.48.refs_0_), channel_id=1, source_target_pairs={{0,2},{1,3},{2,0},{3,1},{4,6},{5,7},{6,4},{7,5},{8,10},{9,11},{10,... | collective-permute-start | bytes 24584 | tf_op jit(solution)/shard_map/ppermute | solution.py:23
  21.9 0.3 collective-permute-start.5
  22.1 1.9 %collective-permute-done.4.refs_2_ = f32[8,256]{1,0:T(8,128)S(1)} collective-permute-done((f32[8,256]{1,0:T(8,128)S(1)}, f32[8,256]{1,0:T(8,128)S(1)}, u32[]{:S(2)}, u32[]{:S(2)}) %collective-permute-start.4) | collective-permute-done | bytes 8224 | tf_op jit(solution)/shard_map/ppermute | solution.py:23
  24.0 1.0 collective-permute-done.5.refs_3_
  25.0 0.7 shard_map.122
  25.7 5.4 %collective-permute-start.31 = (bf16[128,512]{1,0:T(8,128)(2,1)S(1)}, bf16[128,512]{1,0:T(8,128)(2,1)S(1)}, u32[]{:S(2)}, u32[]{:S(2)}) collective-permute-start(bf16[128,512]{1,0:T(8,128)(2,1)S(1)} %get-tuple-element.74), channel_id=1, source_target_pairs={{0,24},{4,28},{8,16},{12,20},{16,8},{20,12},{24,0},{28,4},{1,25},{... | collective-permute-start | bytes 393224 | tf_op jit(solution)/shard_map/ppermute | solution.py:23
  31.0 0.3 collective-permute-start.32
  31.3 0.8 collective-permute-start.22
  32.1 2.9 %collective-permute-start.23 = (bf16[128,512]{1,0:T(8,128)(2,1)S(1)}, bf16[128,512]{1,0:T(8,128)(2,1)S(1)}, u32[]{:S(2)}, u32[]{:S(2)}) collective-permute-start(bf16[128,512]{1,0:T(8,128)(2,1)S(1)} %get-tuple-element.67), channel_id=1, source_target_pairs={{0,20},{4,16},{8,28},{12,24},{16,4},{20,0},{24,12},{28,8},{1,21},{... | collective-permute-start | bytes 393224 | tf_op jit(solution)/shard_map/ppermute | solution.py:23
  34.9 1.4 collective-permute-start.13
  36.3 10.3 %collective-permute-start.14 = (bf16[128,512]{1,0:T(8,128)(2,1)S(1)}, bf16[128,512]{1,0:T(8,128)(2,1)S(1)}, u32[]{:S(2)}, u32[]{:S(2)}) collective-permute-start(bf16[128,512]{1,0:T(8,128)(2,1)S(1)} %get-tuple-element.59), channel_id=1, source_target_pairs={{0,12},{4,8},{8,4},{12,0},{16,28},{20,24},{24,20},{28,16},{1,13},{... | collective-permute-start | bytes 393224 | tf_op jit(solution)/shard_map/ppermute | solution.py:23
  46.7 1.4 collective-permute-start.6
  48.1 3.7 %collective-permute-done.22.refs_0_ = bf16[128,512]{1,0:T(8,128)(2,1)S(1)} collective-permute-done((bf16[128,512]{1,0:T(8,128)(2,1)S(1)}, bf16[128,512]{1,0:T(8,128)(2,1)S(1)}, u32[]{:S(2)}, u32[]{:S(2)}) %collective-permute-start.22) | collective-permute-done | bytes 131104 | tf_op jit(solution)/shard_map/ppermute | solution.py:23
  51.8 0.6 collective-permute-start.33
  52.4 1.5 %collective-permute-done.23.refs_1_ = bf16[128,512]{1,0:T(8,128)(2,1)S(1)} collective-permute-done((bf16[128,512]{1,0:T(8,128)(2,1)S(1)}, bf16[128,512]{1,0:T(8,128)(2,1)S(1)}, u32[]{:S(2)}, u32[]{:S(2)}) %collective-permute-start.23) | collective-permute-done | bytes 131104 | tf_op jit(solution)/shard_map/ppermute | solution.py:23
  54.0 0.6 collective-permute-start.24
  54.6 0.3 collective-permute-done.14.refs_1_
  54.9 0.5 collective-permute-done.6.refs_1_
  55.4 1.0 collective-permute-start.15
  56.4 3.3 %collective-permute-done.33.refs_1_ = bf16[256,512]{1,0:T(8,128)(2,1)S(1)} collective-permute-done((bf16[256,512]{1,0:T(8,128)(2,1)S(1)}, bf16[256,512]{1,0:T(8,128)(2,1)S(1)}, u32[]{:S(2)}, u32[]{:S(2)}) %collective-permute-start.33) | collective-permute-done | bytes 262176 | tf_op jit(solution)/shard_map/ppermute | solution.py:23
  59.7 0.6 collective-permute-start.16
  60.3 5.0 %collective-permute-done.24.refs_1_ = bf16[256,512]{1,0:T(8,128)(2,1)S(1)} collective-permute-done((bf16[256,512]{1,0:T(8,128)(2,1)S(1)}, bf16[256,512]{1,0:T(8,128)(2,1)S(1)}, u32[]{:S(2)}, u32[]{:S(2)}) %collective-permute-start.24) | collective-permute-done | bytes 262176 | tf_op jit(solution)/shard_map/ppermute | solution.py:23
  65.3 0.5 collective-permute-start.7
  65.9 5.1 %shard_map.136 = (bf16[256,1024]{1,0:T(8,128)(2,1)S(1)}, bf16[256,1024]{1,0:T(8,128)(2,1)S(1)}) custom-call(bf16[256,512]{1,0:T(8,128)(2,1)S(1)} %shard_map.135.refs_0_, bf16[256,512]{1,0:T(8,128)(2,1)S(1)} %collective-permute-done.33.refs_1_, bf16[256,512]{1,0:T(8,128)(2,1)S(1)} %collective-permute-done.34.refs_2_, ...), custom_call_target="tpu_custom_call" | custom-call | flops 4429185024 | tf_op jit(solution)/shard_map/pallas_call | solution.py:36
  71.1 0.5 collective-permute-start.8
  71.7 3.6 %collective-permute-done.7.refs_1_ = bf16[256,512]{1,0:T(8,128)(2,1)S(1)} collective-permute-done((bf16[256,512]{1,0:T(8,128)(2,1)S(1)}, bf16[256,512]{1,0:T(8,128)(2,1)S(1)}, u32[]{:S(2)}, u32[]{:S(2)}) %collective-permute-start.7) | collective-permute-done | bytes 262176 | tf_op jit(solution)/shard_map/ppermute | solution.py:23
  75.3 0.5 collective-permute-start.36
  75.8 5.1 %shard_map.132 = (bf16[256,1024]{1,0:T(8,128)(2,1)S(1)}, bf16[256,1024]{1,0:T(8,128)(2,1)S(1)}) custom-call(bf16[256,512]{1,0:T(8,128)(2,1)S(1)} %shard_map.131.refs_0_, bf16[256,512]{1,0:T(8,128)(2,1)S(1)} %collective-permute-done.24.refs_1_, bf16[256,512]{1,0:T(8,128)(2,1)S(1)} %collective-permute-done.25.refs_2_, ...), custom_call_target="tpu_custom_call" | custom-call | flops 4429185024 | tf_op jit(solution)/shard_map/pallas_call | solution.py:36
  80.9 0.3 collective-permute-start.27
  81.2 5.1 %shard_map.128 = (bf16[256,1024]{1,0:T(8,128)(2,1)S(1)}, bf16[256,1024]{1,0:T(8,128)(2,1)S(1)}) custom-call(bf16[256,512]{1,0:T(8,128)(2,1)S(1)} %shard_map.127.refs_0_, bf16[256,512]{1,0:T(8,128)(2,1)S(1)} %collective-permute-done.15.refs_1_, bf16[256,512]{1,0:T(8,128)(2,1)S(1)} %collective-permute-done.16.refs_2_, ...), custom_call_target="tpu_custom_call" | custom-call | flops 4429185024 | tf_op jit(solution)/shard_map/pallas_call | solution.py:36
  86.4 0.6 collective-permute-start.18
  86.9 5.1 %shard_map.124 = (bf16[256,1024]{1,0:T(8,128)(2,1)S(1)}, bf16[256,1024]{1,0:T(8,128)(2,1)S(1)}) custom-call(bf16[256,512]{1,0:T(8,128)(2,1)S(1)} %shard_map.123.refs_0_, bf16[256,512]{1,0:T(8,128)(2,1)S(1)} %collective-permute-done.7.refs_1_, bf16[256,512]{1,0:T(8,128)(2,1)S(1)} %collective-permute-done.8.refs_2_, ...), custom_call_target="tpu_custom_call" | custom-call | flops 4429185024 | tf_op jit(solution)/shard_map/pallas_call | solution.py:36
  92.3 0.6 collective-permute-start.37
  93.0 1.6 %collective-permute-start.28 = (bf16[256,512]{1,0:T(8,128)(2,1)S(1)}, bf16[256,512]{1,0:T(8,128)(2,1)S(1)}, u32[]{:S(2)}, u32[]{:S(2)}) collective-permute-start(bf16[256,512]{1,0:T(8,128)(2,1)S(1)} %get-tuple-element.71), channel_id=1, source_target_pairs={{0,2},{1,3},{2,0},{3,1},{4,6},{5,7},{6,4},{7,5},{8,10},{9,11},{10,... | collective-permute-start | bytes 786440 | tf_op jit(solution)/shard_map/ppermute | solution.py:23
  94.7 0.6 collective-permute-start.19
  95.5 1.6 %collective-permute-start.11 = (bf16[256,512]{1,0:T(8,128)(2,1)S(1)}, bf16[256,512]{1,0:T(8,128)(2,1)S(1)}, u32[]{:S(2)}, u32[]{:S(2)}) collective-permute-start(bf16[256,512]{1,0:T(8,128)(2,1)S(1)} %get-tuple-element.55), channel_id=1, source_target_pairs={{0,2},{1,3},{2,0},{3,1},{4,6},{5,7},{6,4},{7,5},{8,10},{9,11},{10,... | collective-permute-start | bytes 786440 | tf_op jit(solution)/shard_map/ppermute | solution.py:23
  97.0 4.5 %collective-permute-done.37.refs_1_ = bf16[256,512]{1,0:T(8,128)(2,1)S(1)} collective-permute-done((bf16[256,512]{1,0:T(8,128)(2,1)S(1)}, bf16[256,512]{1,0:T(8,128)(2,1)S(1)}, u32[]{:S(2)}, u32[]{:S(2)}) %collective-permute-start.37) | collective-permute-done | bytes 262176 | tf_op jit(solution)/shard_map/ppermute | solution.py:23
  101.6 2.8 %collective-permute-start.38 = (bf16[128,512]{1,0:T(8,128)(2,1)S(1)}, bf16[128,512]{1,0:T(8,128)(2,1)S(1)}, u32[]{:S(2)}, u32[]{:S(2)}) collective-permute-start(bf16[128,512]{1,0:T(8,128)(2,1)S(1)} %get-tuple-element.80), channel_id=1, source_target_pairs={{0,24},{4,28},{8,16},{12,20},{16,8},{20,12},{24,0},{28,4},{1,25},{... | collective-permute-start | bytes 393224 | tf_op jit(solution)/shard_map/ppermute | solution.py:23
  104.4 1.1 collective-permute-start.39
  105.5 1.6 %collective-permute-done.28.refs_1_ = bf16[256,512]{1,0:T(8,128)(2,1)S(1)} collective-permute-done((bf16[256,512]{1,0:T(8,128)(2,1)S(1)}, bf16[256,512]{1,0:T(8,128)(2,1)S(1)}, u32[]{:S(2)}, u32[]{:S(2)}) %collective-permute-start.28) | collective-permute-done | bytes 262176 | tf_op jit(solution)/shard_map/ppermute | solution.py:23
  107.2 0.6 collective-permute-start.29
  107.8 5.0 %collective-permute-done.19.refs_1_ = bf16[256,512]{1,0:T(8,128)(2,1)S(1)} collective-permute-done((bf16[256,512]{1,0:T(8,128)(2,1)S(1)}, bf16[256,512]{1,0:T(8,128)(2,1)S(1)}, u32[]{:S(2)}, u32[]{:S(2)}) %collective-permute-start.19) | collective-permute-done | bytes 262176 | tf_op jit(solution)/shard_map/ppermute | solution.py:23
  112.8 0.4 collective-permute-start.30
  113.2 4.7 %collective-permute-done.11.refs_1_ = bf16[256,512]{1,0:T(8,128)(2,1)S(1)} collective-permute-done((bf16[256,512]{1,0:T(8,128)(2,1)S(1)}, bf16[256,512]{1,0:T(8,128)(2,1)S(1)}, u32[]{:S(2)}, u32[]{:S(2)}) %collective-permute-start.11) | collective-permute-done | bytes 262176 | tf_op jit(solution)/shard_map/ppermute | solution.py:23
  118.0 2.1 %collective-permute-start.21 = (bf16[128,512]{1,0:T(8,128)(2,1)S(1)}, bf16[128,512]{1,0:T(8,128)(2,1)S(1)}, u32[]{:S(2)}, u32[]{:S(2)}) collective-permute-start(bf16[128,512]{1,0:T(8,128)(2,1)S(1)} %get-tuple-element.65), channel_id=1, source_target_pairs={{0,12},{4,8},{8,4},{12,0},{16,28},{20,24},{24,20},{28,16},{1,13},{... | collective-permute-start | bytes 393224 | tf_op jit(solution)/shard_map/ppermute | solution.py:23
  120.1 1.4 %collective-permute-start.12 = (bf16[128,512]{1,0:T(8,128)(2,1)S(1)}, bf16[128,512]{1,0:T(8,128)(2,1)S(1)}, u32[]{:S(2)}, u32[]{:S(2)}) collective-permute-start(bf16[128,512]{1,0:T(8,128)(2,1)S(1)} %get-tuple-element.57), channel_id=1, source_target_pairs={{0,4},{4,0},{8,12},{12,8},{16,20},{20,16},{24,28},{28,24},{1,5},{5... | collective-permute-start | bytes 393224 | tf_op jit(solution)/shard_map/ppermute | solution.py:23
  121.6 2.4 %collective-permute-done.29.refs_4_ = bf16[128,512]{1,0:T(8,128)(2,1)S(1)} collective-permute-done((bf16[128,512]{1,0:T(8,128)(2,1)S(1)}, bf16[128,512]{1,0:T(8,128)(2,1)S(1)}, u32[]{:S(2)}, u32[]{:S(2)}) %collective-permute-start.29) | collective-permute-done | bytes 131104 | tf_op jit(solution)/shard_map/ppermute | solution.py:23
  123.9 1.8 %collective-permute-done.30.refs_5_ = bf16[128,512]{1,0:T(8,128)(2,1)S(1)} collective-permute-done((bf16[128,512]{1,0:T(8,128)(2,1)S(1)}, bf16[128,512]{1,0:T(8,128)(2,1)S(1)}, u32[]{:S(2)}, u32[]{:S(2)}) %collective-permute-start.30) | collective-permute-done | bytes 131104 | tf_op jit(solution)/shard_map/ppermute | solution.py:23
  125.7 2.3 %collective-permute-done.20.refs_2_ = bf16[128,512]{1,0:T(8,128)(2,1)S(1)} collective-permute-done((bf16[128,512]{1,0:T(8,128)(2,1)S(1)}, bf16[128,512]{1,0:T(8,128)(2,1)S(1)}, u32[]{:S(2)}, u32[]{:S(2)}) %collective-permute-start.20) | collective-permute-done | bytes 131104 | tf_op jit(solution)/shard_map/ppermute | solution.py:23
  128.1 2.5 %collective-permute-done.21.refs_3_ = bf16[128,512]{1,0:T(8,128)(2,1)S(1)} collective-permute-done((bf16[128,512]{1,0:T(8,128)(2,1)S(1)}, bf16[128,512]{1,0:T(8,128)(2,1)S(1)}, u32[]{:S(2)}, u32[]{:S(2)}) %collective-permute-start.21) | collective-permute-done | bytes 131104 | tf_op jit(solution)/shard_map/ppermute | solution.py:23
  130.6 1.5 %shard_map.139.refs_0_ = bf16[256,512]{1,0:T(8,128)(2,1)S(1)} custom-call(bf16[128,512]{1,0:T(8,128)(2,1)S(1)} %get-tuple-element.56.refs_0_, bf16[128,512]{1,0:T(8,128)(2,1)S(1)} %collective-permute-done.12.refs_1_, bf16[128,512]{1,0:T(8,128)(2,1)S(1)} %collective-permute-done.20.refs_2_, bf16[128,512]{1,0:T(8,128)(2,1)S(1)} %collective-permute-done.21.refs_3_, ...), custom_call_target="tpu_custom_call" | custom-call | flops 536870912 | tf_op jit(solution)/shard_map/pallas_call | solution.py:36
  132.1 0.6 collective-permute-start.40
  132.7 7.2 %collective-permute-done.40.refs_1_ = bf16[256,512]{1,0:T(8,128)(2,1)S(1)} collective-permute-done((bf16[256,512]{1,0:T(8,128)(2,1)S(1)}, bf16[256,512]{1,0:T(8,128)(2,1)S(1)}, u32[]{:S(2)}, u32[]{:S(2)}) %collective-permute-start.40) | collective-permute-done | bytes 262176 | tf_op jit(solution)/shard_map/ppermute | solution.py:23
  139.9 1.5 %collective-permute-done.42.refs_3_ = bf16[256,512]{1,0:T(8,128)(2,1)S(1)} collective-permute-done((bf16[256,512]{1,0:T(8,128)(2,1)S(1)}, bf16[256,512]{1,0:T(8,128)(2,1)S(1)}, u32[]{:S(2)}, u32[]{:S(2)}) %collective-permute-start.42) | collective-permute-done | bytes 262176 | tf_op jit(solution)/shard_map/ppermute | solution.py:23
  141.4 1.7 %shard_map.140 = bf16[256,2048]{1,0:T(8,128)(2,1)} custom-call(bf16[256,512]{1,0:T(8,128)(2,1)S(1)} %shard_map.139.refs_0_, bf16[256,512]{1,0:T(8,128)(2,1)S(1)} %collective-permute-done.40.refs_1_, bf16[256,512]{1,0:T(8,128)(2,1)S(1)} %collective-permute-done.41.refs_2_, bf16[256,512]{1,0:T(8,128)(2,1)S(1)} %collective-permute-done.42.refs_3_, ...), custom_call_target="tpu_custom_call" | custom-call | flops 3000000000 | tf_op jit(solution)/shard_map/pallas_call | solution.py:36
  (78 shorter events, 1.4 us)
Async XLA Ops:
  0.0 0.9 copy-start.2
  1.0 0.7 copy-start.8
  1.6 6.6 %copy-start = (bf16[512,2048]{1,0:T(8,128)(2,1)S(1)}, bf16[512,2048]{1,0:T(8,128)(2,1)}, u32[]{:S(2)}) copy-start(bf16[512,2048]{1,0:T(8,128)(2,1)} %weights.1) | copy-start | bytes 6291460
  1.6 6.6 %copy-start.5 = (f32[512]{0:T(512)S(1)}, f32[512]{0:T(512)}, u32[]{:S(2)}) copy-start(f32[512]{0:T(512)} %param.14) | copy-start | bytes 6148
  1.6 6.6 %collective-permute-start = (bf16[32,512]{1,0:T(8,128)(2,1)S(1)}, bf16[32,512]{1,0:T(8,128)(2,1)S(1)}, u32[]{:S(2)}, u32[]{:S(2)}) collective-permute-start(bf16[32,512]{1,0:T(8,128)(2,1)S(1)} %shard_map.118), channel_id=1, source_target_pairs={{0,4},{4,8},{8,12},{12,16},{16,20},{20,24},{24,28},{1,5},{5,9},{9,... | collective-permute-start | bytes 98312 | tf_op jit(solution)/shard_map/ppermute | solution.py:279
  9.4 2.0 %collective-permute-start.1 = (bf16[256,1024]{1,0:T(8,128)(2,1)S(1)}, bf16[256,1024]{1,0:T(8,128)(2,1)S(1)}, u32[]{:S(2)}, u32[]{:S(2)}) collective-permute-start(bf16[256,1024]{1,0:T(8,128)(2,1)S(1)} %get-tuple-element.45), channel_id=1, source_target_pairs={{0,1},{1,0},{2,3},{3,2},{4,5},{5,4},{6,7},{7,6},{8,9},{9,8},{10,11... | collective-permute-start | bytes 1572872 | tf_op jit(solution)/shard_map/ppermute | solution.py:23
  11.4 8.5 %copy-start.1 = (bf16[256,2048]{1,0:T(8,128)(2,1)S(1)}, bf16[256,2048]{1,0:T(8,128)(2,1)}, u32[]{:S(2)}) copy-start(bf16[256,2048]{1,0:T(8,128)(2,1)} %refs_2_.1) | copy-start | bytes 3145732
  11.5 8.4 %collective-permute-start.2 = (bf16[256,512]{1,0:T(8,128)(2,1)S(1)}, bf16[256,512]{1,0:T(8,128)(2,1)S(1)}, u32[]{:S(2)}, u32[]{:S(2)}) collective-permute-start(bf16[256,512]{1,0:T(8,128)(2,1)S(1)} %get-tuple-element.47), channel_id=1, source_target_pairs={{0,2},{1,3},{2,0},{3,1},{4,6},{5,7},{6,4},{7,5},{8,10},{9,11},{10,... | collective-permute-start | bytes 786440 | tf_op jit(solution)/shard_map/ppermute | solution.py:23
  19.9 5.0 %copy-start.3 = (f32[2048]{0:T(1024)S(1)}, f32[2048]{0:T(1024)}, u32[]{:S(2)}) copy-start(f32[2048]{0:T(1024)} %param.17) | copy-start | bytes 24580
  19.9 5.0 %copy-start.6 = (s32[256,2]{0,1:T(2,128)S(1)}, s32[256,2]{0,1:T(2,128)}, u32[]{:S(2)}) copy-start(s32[256,2]{0,1:T(2,128)} %param.18) | copy-start | bytes 6148
  20.2 1.9 %collective-permute-start.3 = (f32[8,256]{1,0:T(8,128)S(1)}, f32[8,256]{1,0:T(8,128)S(1)}, u32[]{:S(2)}, u32[]{:S(2)}) collective-permute-start(f32[8,256]{1,0:T(8,128)S(1)} %get-tuple-element.48.refs_0_), channel_id=1, source_target_pairs={{0,1},{1,0},{2,3},{3,2},{4,5},{5,4},{6,7},{7,6},{8,9},{9,8},{10,11... | collective-permute-start | bytes 24584 | tf_op jit(solution)/shard_map/ppermute | solution.py:23
  20.3 3.7 %collective-permute-start.4 = (f32[8,256]{1,0:T(8,128)S(1)}, f32[8,256]{1,0:T(8,128)S(1)}, u32[]{:S(2)}, u32[]{:S(2)}) collective-permute-start(f32[8,256]{1,0:T(8,128)S(1)} %get-tuple-element.48.refs_0_), channel_id=1, source_target_pairs={{0,2},{1,3},{2,0},{3,1},{4,6},{5,7},{6,4},{7,5},{8,10},{9,11},{10,... | collective-permute-start | bytes 24584 | tf_op jit(solution)/shard_map/ppermute | solution.py:23
  21.9 3.1 %collective-permute-start.5 = (f32[8,256]{1,0:T(8,128)S(1)}, f32[8,256]{1,0:T(8,128)S(1)}, u32[]{:S(2)}, u32[]{:S(2)}) collective-permute-start(f32[8,256]{1,0:T(8,128)S(1)} %get-tuple-element.48.refs_0_), channel_id=1, source_target_pairs={{0,3},{1,2},{2,1},{3,0},{4,7},{5,6},{6,5},{7,4},{8,11},{9,10},{10,... | collective-permute-start | bytes 24584 | tf_op jit(solution)/shard_map/ppermute | solution.py:23
  25.7 10.7 %collective-permute-start.31 = (bf16[128,512]{1,0:T(8,128)(2,1)S(1)}, bf16[128,512]{1,0:T(8,128)(2,1)S(1)}, u32[]{:S(2)}, u32[]{:S(2)}) collective-permute-start(bf16[128,512]{1,0:T(8,128)(2,1)S(1)} %get-tuple-element.74), channel_id=1, source_target_pairs={{0,24},{4,28},{8,16},{12,20},{16,8},{20,12},{24,0},{28,4},{1,25},{... | collective-permute-start | bytes 393224 | tf_op jit(solution)/shard_map/ppermute | solution.py:23
  31.0 15.6 %collective-permute-start.32 = (bf16[128,512]{1,0:T(8,128)(2,1)S(1)}, bf16[128,512]{1,0:T(8,128)(2,1)S(1)}, u32[]{:S(2)}, u32[]{:S(2)}) collective-permute-start(bf16[128,512]{1,0:T(8,128)(2,1)S(1)} %get-tuple-element.75), channel_id=1, source_target_pairs={{0,28},{4,24},{8,20},{12,16},{16,12},{20,8},{24,4},{28,0},{1,29},{... | collective-permute-start | bytes 393224 | tf_op jit(solution)/shard_map/ppermute | solution.py:23
  31.3 20.5 %collective-permute-start.22 = (bf16[128,512]{1,0:T(8,128)(2,1)S(1)}, bf16[128,512]{1,0:T(8,128)(2,1)S(1)}, u32[]{:S(2)}, u32[]{:S(2)}) collective-permute-start(bf16[128,512]{1,0:T(8,128)(2,1)S(1)} %get-tuple-element.66), channel_id=1, source_target_pairs={{0,16},{4,20},{8,24},{12,28},{16,0},{20,4},{24,8},{28,12},{1,17},{... | collective-permute-start | bytes 393224 | tf_op jit(solution)/shard_map/ppermute | solution.py:23
  32.1 21.8 %collective-permute-start.23 = (bf16[128,512]{1,0:T(8,128)(2,1)S(1)}, bf16[128,512]{1,0:T(8,128)(2,1)S(1)}, u32[]{:S(2)}, u32[]{:S(2)}) collective-permute-start(bf16[128,512]{1,0:T(8,128)(2,1)S(1)} %get-tuple-element.67), channel_id=1, source_target_pairs={{0,20},{4,16},{8,28},{12,24},{16,4},{20,0},{24,12},{28,8},{1,21},{... | collective-permute-start | bytes 393224 | tf_op jit(solution)/shard_map/ppermute | solution.py:23
  34.9 19.0 %collective-permute-start.13 = (bf16[128,512]{1,0:T(8,128)(2,1)S(1)}, bf16[128,512]{1,0:T(8,128)(2,1)S(1)}, u32[]{:S(2)}, u32[]{:S(2)}) collective-permute-start(bf16[128,512]{1,0:T(8,128)(2,1)S(1)} %get-tuple-element.58), channel_id=1, source_target_pairs={{0,8},{4,12},{8,0},{12,4},{16,24},{20,28},{24,16},{28,20},{1,9},{5... | collective-permute-start | bytes 393224 | tf_op jit(solution)/shard_map/ppermute | solution.py:23
  36.3 18.5 %collective-permute-start.14 = (bf16[128,512]{1,0:T(8,128)(2,1)S(1)}, bf16[128,512]{1,0:T(8,128)(2,1)S(1)}, u32[]{:S(2)}, u32[]{:S(2)}) collective-permute-start(bf16[128,512]{1,0:T(8,128)(2,1)S(1)} %get-tuple-element.59), channel_id=1, source_target_pairs={{0,12},{4,8},{8,4},{12,0},{16,28},{20,24},{24,20},{28,16},{1,13},{... | collective-permute-start | bytes 393224 | tf_op jit(solution)/shard_map/ppermute | solution.py:23
  46.7 8.7 %collective-permute-start.6 = (bf16[128,512]{1,0:T(8,128)(2,1)S(1)}, bf16[128,512]{1,0:T(8,128)(2,1)S(1)}, u32[]{:S(2)}, u32[]{:S(2)}) collective-permute-start(bf16[128,512]{1,0:T(8,128)(2,1)S(1)} %get-tuple-element.51), channel_id=1, source_target_pairs={{0,4},{4,0},{8,12},{12,8},{16,20},{20,16},{24,28},{28,24},{1,5},{5... | collective-permute-start | bytes 393224 | tf_op jit(solution)/shard_map/ppermute | solution.py:23
  51.8 7.9 %collective-permute-start.33 = (bf16[256,512]{1,0:T(8,128)(2,1)S(1)}, bf16[256,512]{1,0:T(8,128)(2,1)S(1)}, u32[]{:S(2)}, u32[]{:S(2)}) collective-permute-start(bf16[256,512]{1,0:T(8,128)(2,1)S(1)} %shard_map.135.refs_0_), channel_id=1, source_target_pairs={{0,2},{1,3},{2,0},{3,1},{4,6},{5,7},{6,4},{7,5},{8,10},{9,11},{10,... | collective-permute-start | bytes 786440 | tf_op jit(solution)/shard_map/ppermute | solution.py:23
  53.9 5.8 %collective-permute-start.34 = (bf16[256,512]{1,0:T(8,128)(2,1)S(1)}, bf16[256,512]{1,0:T(8,128)(2,1)S(1)}, u32[]{:S(2)}, u32[]{:S(2)}) collective-permute-start(bf16[256,512]{1,0:T(8,128)(2,1)S(1)} %shard_map.135.refs_0_), channel_id=1, source_target_pairs={{0,1},{1,0},{2,3},{3,2},{4,5},{5,4},{6,7},{7,6},{8,9},{9,8},{10,11... | collective-permute-start | bytes 786440 | tf_op jit(solution)/shard_map/ppermute | solution.py:23
  53.9 11.9 %slice-start.2 = ((s8[5767168]{0:T(1024)(128)(4,1)}), s8[4194304]{0:T(1024)(128)(4,1)S(1)}, s32[]{:S(2)}) async-start(s8[5767168]{0:T(1024)(128)(4,1)} %bitcast.15), calls=%async_computation.2 | async-start | bytes 8388608
  53.9 11.9 %slice-start.4 = ((s8[5767168]{0:T(1024)(128)(4,1)}), s8[4194304]{0:T(1024)(128)(4,1)S(1)}, s32[]{:S(2)}) async-start(s8[5767168]{0:T(1024)(128)(4,1)} %bitcast.21), calls=%async_computation.4 | async-start | bytes 8388608
  53.9 11.9 %slice-start.3 = ((s8[5767168]{0:T(1024)(128)(4,1)}), s8[1572864]{0:T(1024)(128)(4,1)S(1)}, s32[]{:S(2)}) async-start(s8[5767168]{0:T(1024)(128)(4,1)} %bitcast.15), calls=%async_computation.3 | async-start | bytes 3145728
  53.9 11.9 %slice-start.5 = ((s8[5767168]{0:T(1024)(128)(4,1)}), s8[1572864]{0:T(1024)(128)(4,1)S(1)}, s32[]{:S(2)}) async-start(s8[5767168]{0:T(1024)(128)(4,1)} %bitcast.21), calls=%async_computation.5 | async-start | bytes 3145728
  54.0 11.3 %collective-permute-start.24 = (bf16[256,512]{1,0:T(8,128)(2,1)S(1)}, bf16[256,512]{1,0:T(8,128)(2,1)S(1)}, u32[]{:S(2)}, u32[]{:S(2)}) collective-permute-start(bf16[256,512]{1,0:T(8,128)(2,1)S(1)} %shard_map.131.refs_0_), channel_id=1, source_target_pairs={{0,2},{1,3},{2,0},{3,1},{4,6},{5,7},{6,4},{7,5},{8,10},{9,11},{10,... | collective-permute-start | bytes 786440 | tf_op jit(solution)/shard_map/ppermute | solution.py:23
  54.8 16.2 %collective-permute-start.25 = (bf16[256,512]{1,0:T(8,128)(2,1)S(1)}, bf16[256,512]{1,0:T(8,128)(2,1)S(1)}, u32[]{:S(2)}, u32[]{:S(2)}) collective-permute-start(bf16[256,512]{1,0:T(8,128)(2,1)S(1)} %shard_map.131.refs_0_), channel_id=1, source_target_pairs={{0,1},{1,0},{2,3},{3,2},{4,5},{5,4},{6,7},{7,6},{8,9},{9,8},{10,11... | collective-permute-start | bytes 786440 | tf_op jit(solution)/shard_map/ppermute | solution.py:23
  54.9 11.0 %slice-start = ((s8[5767168]{0:T(1024)(128)(4,1)}), s8[4194304]{0:T(1024)(128)(4,1)S(1)}, s32[]{:S(2)}) async-start(s8[5767168]{0:T(1024)(128)(4,1)} %bitcast.9), calls=%async_computation | async-start | bytes 8388608
  55.4 16.3 %collective-permute-start.15 = (bf16[256,512]{1,0:T(8,128)(2,1)S(1)}, bf16[256,512]{1,0:T(8,128)(2,1)S(1)}, u32[]{:S(2)}, u32[]{:S(2)}) collective-permute-start(bf16[256,512]{1,0:T(8,128)(2,1)S(1)} %shard_map.127.refs_0_), channel_id=1, source_target_pairs={{0,2},{1,3},{2,0},{3,1},{4,6},{5,7},{6,4},{7,5},{8,10},{9,11},{10,... | collective-permute-start | bytes 786440 | tf_op jit(solution)/shard_map/ppermute | solution.py:23
  59.7 6.1 %collective-permute-start.35 = (bf16[256,512]{1,0:T(8,128)(2,1)S(1)}, bf16[256,512]{1,0:T(8,128)(2,1)S(1)}, u32[]{:S(2)}, u32[]{:S(2)}) collective-permute-start(bf16[256,512]{1,0:T(8,128)(2,1)S(1)} %collective-permute-done.33.refs_1_), channel_id=1, source_target_pairs={{0,1},{1,0},{2,3},{3,2},{4,5},{5,4},{6,7},{7,6},{8,9},{9,8},{10,11... | collective-permute-start | bytes 786440 | tf_op jit(solution)/shard_map/ppermute | solution.py:23
  59.7 6.2 %slice-start.1 = ((s8[5767168]{0:T(1024)(128)(4,1)}), s8[1572864]{0:T(1024)(128)(4,1)S(1)}, s32[]{:S(2)}) async-start(s8[5767168]{0:T(1024)(128)(4,1)} %bitcast.9), calls=%async_computation.1 | async-start | bytes 3145728
  59.7 21.2 %collective-permute-start.16 = (bf16[256,512]{1,0:T(8,128)(2,1)S(1)}, bf16[256,512]{1,0:T(8,128)(2,1)S(1)}, u32[]{:S(2)}, u32[]{:S(2)}) collective-permute-start(bf16[256,512]{1,0:T(8,128)(2,1)S(1)} %shard_map.127.refs_0_), channel_id=1, source_target_pairs={{0,1},{1,0},{2,3},{3,2},{4,5},{5,4},{6,7},{7,6},{8,9},{9,8},{10,11... | collective-permute-start | bytes 786440 | tf_op jit(solution)/shard_map/ppermute | solution.py:23
  65.3 10.0 %collective-permute-start.7 = (bf16[256,512]{1,0:T(8,128)(2,1)S(1)}, bf16[256,512]{1,0:T(8,128)(2,1)S(1)}, u32[]{:S(2)}, u32[]{:S(2)}) collective-permute-start(bf16[256,512]{1,0:T(8,128)(2,1)S(1)} %shard_map.123.refs_0_), channel_id=1, source_target_pairs={{0,2},{1,3},{2,0},{3,1},{4,6},{5,7},{6,4},{7,5},{8,10},{9,11},{10,... | collective-permute-start | bytes 786440 | tf_op jit(solution)/shard_map/ppermute | solution.py:23
  65.8 9.5 %collective-permute-start.26 = (bf16[256,512]{1,0:T(8,128)(2,1)S(1)}, bf16[256,512]{1,0:T(8,128)(2,1)S(1)}, u32[]{:S(2)}, u32[]{:S(2)}) collective-permute-start(bf16[256,512]{1,0:T(8,128)(2,1)S(1)} %collective-permute-done.24.refs_1_), channel_id=1, source_target_pairs={{0,1},{1,0},{2,3},{3,2},{4,5},{5,4},{6,7},{7,6},{8,9},{9,8},{10,11... | collective-permute-start | bytes 786440 | tf_op jit(solution)/shard_map/ppermute | solution.py:23
  71.1 15.9 %collective-permute-start.8 = (bf16[256,512]{1,0:T(8,128)(2,1)S(1)}, bf16[256,512]{1,0:T(8,128)(2,1)S(1)}, u32[]{:S(2)}, u32[]{:S(2)}) collective-permute-start(bf16[256,512]{1,0:T(8,128)(2,1)S(1)} %shard_map.123.refs_0_), channel_id=1, source_target_pairs={{0,1},{1,0},{2,3},{3,2},{4,5},{5,4},{6,7},{7,6},{8,9},{9,8},{10,11... | collective-permute-start | bytes 786440 | tf_op jit(solution)/shard_map/ppermute | solution.py:23
  71.6 9.6 %collective-permute-start.17 = (bf16[256,512]{1,0:T(8,128)(2,1)S(1)}, bf16[256,512]{1,0:T(8,128)(2,1)S(1)}, u32[]{:S(2)}, u32[]{:S(2)}) collective-permute-start(bf16[256,512]{1,0:T(8,128)(2,1)S(1)} %collective-permute-done.15.refs_1_), channel_id=1, source_target_pairs={{0,1},{1,0},{2,3},{3,2},{4,5},{5,4},{6,7},{7,6},{8,9},{9,8},{10,11... | collective-permute-start | bytes 786440 | tf_op jit(solution)/shard_map/ppermute | solution.py:23
  75.3 11.7 %collective-permute-start.9 = (bf16[256,512]{1,0:T(8,128)(2,1)S(1)}, bf16[256,512]{1,0:T(8,128)(2,1)S(1)}, u32[]{:S(2)}, u32[]{:S(2)}) collective-permute-start(bf16[256,512]{1,0:T(8,128)(2,1)S(1)} %collective-permute-done.7.refs_1_), channel_id=1, source_target_pairs={{0,1},{1,0},{2,3},{3,2},{4,5},{5,4},{6,7},{7,6},{8,9},{9,8},{10,11... | collective-permute-start | bytes 786440 | tf_op jit(solution)/shard_map/ppermute | solution.py:23
  75.3 16.9 %collective-permute-start.36 = (bf16[256,1024]{1,0:T(8,128)(2,1)S(1)}, bf16[256,1024]{1,0:T(8,128)(2,1)S(1)}, u32[]{:S(2)}, u32[]{:S(2)}) collective-permute-start(bf16[256,1024]{1,0:T(8,128)(2,1)S(1)} %get-tuple-element.77), channel_id=1, source_target_pairs={{0,1},{1,0},{2,3},{3,2},{4,5},{5,4},{6,7},{7,6},{8,9},{9,8},{10,11... | collective-permute-start | bytes 1572872 | tf_op jit(solution)/shard_map/ppermute | solution.py:23
  80.9 12.0 %collective-permute-start.27 = (bf16[256,1024]{1,0:T(8,128)(2,1)S(1)}, bf16[256,1024]{1,0:T(8,128)(2,1)S(1)}, u32[]{:S(2)}, u32[]{:S(2)}) collective-permute-start(bf16[256,1024]{1,0:T(8,128)(2,1)S(1)} %get-tuple-element.69), channel_id=1, source_target_pairs={{0,1},{1,0},{2,3},{3,2},{4,5},{5,4},{6,7},{7,6},{8,9},{9,8},{10,11... | collective-permute-start | bytes 1572872 | tf_op jit(solution)/shard_map/ppermute | solution.py:23
  86.4 8.2 %collective-permute-start.18 = (bf16[256,1024]{1,0:T(8,128)(2,1)S(1)}, bf16[256,1024]{1,0:T(8,128)(2,1)S(1)}, u32[]{:S(2)}, u32[]{:S(2)}) collective-permute-start(bf16[256,1024]{1,0:T(8,128)(2,1)S(1)} %get-tuple-element.61), channel_id=1, source_target_pairs={{0,1},{1,0},{2,3},{3,2},{4,5},{5,4},{6,7},{7,6},{8,9},{9,8},{10,11... | collective-permute-start | bytes 1572872 | tf_op jit(solution)/shard_map/ppermute | solution.py:23
  92.1 3.2 %collective-permute-start.10 = (bf16[256,1024]{1,0:T(8,128)(2,1)S(1)}, bf16[256,1024]{1,0:T(8,128)(2,1)S(1)}, u32[]{:S(2)}, u32[]{:S(2)}) collective-permute-start(bf16[256,1024]{1,0:T(8,128)(2,1)S(1)} %get-tuple-element.53), channel_id=1, source_target_pairs={{0,1},{1,0},{2,3},{3,2},{4,5},{5,4},{6,7},{7,6},{8,9},{9,8},{10,11... | collective-permute-start | bytes 1572872 | tf_op jit(solution)/shard_map/ppermute | solution.py:23
  92.3 9.2 %collective-permute-start.37 = (bf16[256,512]{1,0:T(8,128)(2,1)S(1)}, bf16[256,512]{1,0:T(8,128)(2,1)S(1)}, u32[]{:S(2)}, u32[]{:S(2)}) collective-permute-start(bf16[256,512]{1,0:T(8,128)(2,1)S(1)} %get-tuple-element.79), channel_id=1, source_target_pairs={{0,2},{1,3},{2,0},{3,1},{4,6},{5,7},{6,4},{7,5},{8,10},{9,11},{10,... | collective-permute-start | bytes 786440 | tf_op jit(solution)/shard_map/ppermute | solution.py:23
  93.0 14.1 %collective-permute-start.28 = (bf16[256,512]{1,0:T(8,128)(2,1)S(1)}, bf16[256,512]{1,0:T(8,128)(2,1)S(1)}, u32[]{:S(2)}, u32[]{:S(2)}) collective-permute-start(bf16[256,512]{1,0:T(8,128)(2,1)S(1)} %get-tuple-element.71), channel_id=1, source_target_pairs={{0,2},{1,3},{2,0},{3,1},{4,6},{5,7},{6,4},{7,5},{8,10},{9,11},{10,... | collective-permute-start | bytes 786440 | tf_op jit(solution)/shard_map/ppermute | solution.py:23
  94.7 18.1 %collective-permute-start.19 = (bf16[256,512]{1,0:T(8,128)(2,1)S(1)}, bf16[256,512]{1,0:T(8,128)(2,1)S(1)}, u32[]{:S(2)}, u32[]{:S(2)}) collective-permute-start(bf16[256,512]{1,0:T(8,128)(2,1)S(1)} %get-tuple-element.63), channel_id=1, source_target_pairs={{0,2},{1,3},{2,0},{3,1},{4,6},{5,7},{6,4},{7,5},{8,10},{9,11},{10,... | collective-permute-start | bytes 786440 | tf_op jit(solution)/shard_map/ppermute | solution.py:23
  95.5 22.5 %collective-permute-start.11 = (bf16[256,512]{1,0:T(8,128)(2,1)S(1)}, bf16[256,512]{1,0:T(8,128)(2,1)S(1)}, u32[]{:S(2)}, u32[]{:S(2)}) collective-permute-start(bf16[256,512]{1,0:T(8,128)(2,1)S(1)} %get-tuple-element.55), channel_id=1, source_target_pairs={{0,2},{1,3},{2,0},{3,1},{4,6},{5,7},{6,4},{7,5},{8,10},{9,11},{10,... | collective-permute-start | bytes 786440 | tf_op jit(solution)/shard_map/ppermute | solution.py:23
  101.6 16.4 %collective-permute-start.38 = (bf16[128,512]{1,0:T(8,128)(2,1)S(1)}, bf16[128,512]{1,0:T(8,128)(2,1)S(1)}, u32[]{:S(2)}, u32[]{:S(2)}) collective-permute-start(bf16[128,512]{1,0:T(8,128)(2,1)S(1)} %get-tuple-element.80), channel_id=1, source_target_pairs={{0,24},{4,28},{8,16},{12,20},{16,8},{20,12},{24,0},{28,4},{1,25},{... | collective-permute-start | bytes 393224 | tf_op jit(solution)/shard_map/ppermute | solution.py:23
  104.4 15.7 %collective-permute-start.39 = (bf16[128,512]{1,0:T(8,128)(2,1)S(1)}, bf16[128,512]{1,0:T(8,128)(2,1)S(1)}, u32[]{:S(2)}, u32[]{:S(2)}) collective-permute-start(bf16[128,512]{1,0:T(8,128)(2,1)S(1)} %get-tuple-element.81), channel_id=1, source_target_pairs={{0,28},{4,24},{8,20},{12,16},{16,12},{20,8},{24,4},{28,0},{1,29},{... | collective-permute-start | bytes 393224 | tf_op jit(solution)/shard_map/ppermute | solution.py:23
  107.2 16.7 %collective-permute-start.29 = (bf16[128,512]{1,0:T(8,128)(2,1)S(1)}, bf16[128,512]{1,0:T(8,128)(2,1)S(1)}, u32[]{:S(2)}, u32[]{:S(2)}) collective-permute-start(bf16[128,512]{1,0:T(8,128)(2,1)S(1)} %get-tuple-element.72), channel_id=1, source_target_pairs={{0,16},{4,20},{8,24},{12,28},{16,0},{20,4},{24,8},{28,12},{1,17},{... | collective-permute-start | bytes 393224 | tf_op jit(solution)/shard_map/ppermute | solution.py:23
  112.8 12.9 %collective-permute-start.30 = (bf16[128,512]{1,0:T(8,128)(2,1)S(1)}, bf16[128,512]{1,0:T(8,128)(2,1)S(1)}, u32[]{:S(2)}, u32[]{:S(2)}) collective-permute-start(bf16[128,512]{1,0:T(8,128)(2,1)S(1)} %get-tuple-element.73), channel_id=1, source_target_pairs={{0,20},{4,16},{8,28},{12,24},{16,4},{20,0},{24,12},{28,8},{1,21},{... | collective-permute-start | bytes 393224 | tf_op jit(solution)/shard_map/ppermute | solution.py:23
  113.2 17.4 %copy-start.7 = (f32[256,2]{0,1:T(2,128)S(1)}, f32[256,2]{0,1:T(2,128)}, u32[]{:S(2)}) copy-start(f32[256,2]{0,1:T(2,128)} %param.19) | copy-start | bytes 6148
  117.9 10.1 %collective-permute-start.20 = (bf16[128,512]{1,0:T(8,128)(2,1)S(1)}, bf16[128,512]{1,0:T(8,128)(2,1)S(1)}, u32[]{:S(2)}, u32[]{:S(2)}) collective-permute-start(bf16[128,512]{1,0:T(8,128)(2,1)S(1)} %get-tuple-element.64), channel_id=1, source_target_pairs={{0,8},{4,12},{8,0},{12,4},{16,24},{20,28},{24,16},{28,20},{1,9},{5... | collective-permute-start | bytes 393224 | tf_op jit(solution)/shard_map/ppermute | solution.py:23
  117.9 23.5 %copy-start.4 = (f32[2048]{0:T(1024)S(1)}, f32[2048]{0:T(1024)}, u32[]{:S(2)}) copy-start(f32[2048]{0:T(1024)} %param.23) | copy-start | bytes 24580
  118.0 12.6 %collective-permute-start.21 = (bf16[128,512]{1,0:T(8,128)(2,1)S(1)}, bf16[128,512]{1,0:T(8,128)(2,1)S(1)}, u32[]{:S(2)}, u32[]{:S(2)}) collective-permute-start(bf16[128,512]{1,0:T(8,128)(2,1)S(1)} %get-tuple-element.65), channel_id=1, source_target_pairs={{0,12},{4,8},{8,4},{12,0},{16,28},{20,24},{24,20},{28,16},{1,13},{... | collective-permute-start | bytes 393224 | tf_op jit(solution)/shard_map/ppermute | solution.py:23
  120.1 10.5 %collective-permute-start.12 = (bf16[128,512]{1,0:T(8,128)(2,1)S(1)}, bf16[128,512]{1,0:T(8,128)(2,1)S(1)}, u32[]{:S(2)}, u32[]{:S(2)}) collective-permute-start(bf16[128,512]{1,0:T(8,128)(2,1)S(1)} %get-tuple-element.57), channel_id=1, source_target_pairs={{0,4},{4,0},{8,12},{12,8},{16,20},{20,16},{24,28},{28,24},{1,5},{5... | collective-permute-start | bytes 393224 | tf_op jit(solution)/shard_map/ppermute | solution.py:23
  132.1 7.8 %collective-permute-start.40 = (bf16[256,512]{1,0:T(8,128)(2,1)S(1)}, bf16[256,512]{1,0:T(8,128)(2,1)S(1)}, u32[]{:S(2)}, u32[]{:S(2)}) collective-permute-start(bf16[256,512]{1,0:T(8,128)(2,1)S(1)} %shard_map.139.refs_0_), channel_id=1, source_target_pairs={{0,2},{1,3},{2,0},{3,1},{4,6},{5,7},{6,4},{7,5},{8,10},{9,11},{10,... | collective-permute-start | bytes 786440 | tf_op jit(solution)/shard_map/ppermute | solution.py:23
  132.7 7.2 %collective-permute-start.41 = (bf16[256,512]{1,0:T(8,128)(2,1)S(1)}, bf16[256,512]{1,0:T(8,128)(2,1)S(1)}, u32[]{:S(2)}, u32[]{:S(2)}) collective-permute-start(bf16[256,512]{1,0:T(8,128)(2,1)S(1)} %shard_map.139.refs_0_), channel_id=1, source_target_pairs={{0,1},{1,0},{2,3},{3,2},{4,5},{5,4},{6,7},{7,6},{8,9},{9,8},{10,11... | collective-permute-start | bytes 786440 | tf_op jit(solution)/shard_map/ppermute | solution.py:23
  139.9 1.5 %collective-permute-start.42 = (bf16[256,512]{1,0:T(8,128)(2,1)S(1)}, bf16[256,512]{1,0:T(8,128)(2,1)S(1)}, u32[]{:S(2)}, u32[]{:S(2)}) collective-permute-start(bf16[256,512]{1,0:T(8,128)(2,1)S(1)} %collective-permute-done.40.refs_1_), channel_id=1, source_target_pairs={{0,1},{1,0},{2,3},{3,2},{4,5},{5,4},{6,7},{7,6},{8,9},{9,8},{10,11... | collective-permute-start | bytes 786440 | tf_op jit(solution)/shard_map/ppermute | solution.py:23
